TPU v7x, 32 devices: a whole 2x2x4 slice. The times are simulated.
32 devices in a mesh: grp: 2 (over x), ep: 16 (over z, y, core).
Axes of the slice: x: 2, y: 2, z: 4, core: 2. Of those that a mesh axis runs over, the one named last changes fastest.
Arguments:
- tokens: bfloat16 [32, 2048], P(('grp', 'ep')), parts along dimension 0, may hold values from -6 to 6
- cache_latent: bfloat16 [32, 3072, 512], P(('grp', 'ep')), parts along dimension 0, may hold values from -6 to 6
- cache_rope: bfloat16 [32, 32, 3072], P(('grp', 'ep')), parts along dimension 0, may hold values from -1000 to 1000
- lengths: int32 [32], P(('grp', 'ep')), parts along dimension 0, may hold values from 384 to 3072, as said below
- w_query: bfloat16 [2048, 1536], P('ep'), may hold values from -0.125 to 0.125
- w_latent: bfloat16 [2048, 512], P('ep'), may hold values from -0.125 to 0.125
- w_rope: bfloat16 [2048, 32], P('ep'), may hold values from -0.125 to 0.125
- w_absorb: bfloat16 [512, 1024], replicated, may hold values from -0.25 to 0.25
- w_value: bfloat16 [512, 1024], replicated, may hold values from -0.25 to 0.25
- w_output: bfloat16 [1024, 2048], P('ep'), may hold values from -0.1875 to 0.1875
- gain_attn: float32 [2048], replicated, may hold values from 0.1 to 1.9
- gain_latent: float32 [512], replicated, may hold values from 0.1 to 1.9
- gain_moe: float32 [2048], replicated, may hold values from 0.1 to 1.9
- routes: int32 [32, 2], P(('grp', 'ep')), parts along dimension 0, may hold values from 0 to 15, all different within a row; in each aligned block of 16 rows (0 to 15, 16 to 31, ...) at most 4 rows name the same one
- route_scores: float32 [32, 2], P(('grp', 'ep')), parts along dimension 0, may hold values from 0.2 to 1
- w_gate: bfloat16 [16, 2048, 512], P('ep'), may hold values from -0.125 to 0.125
- w_up: bfloat16 [16, 2048, 512], P('ep'), may hold values from -0.125 to 0.125
- w_down: bfloat16 [16, 512, 2048], P('ep'), may hold values from -0.25 to 0.25
Outputs:
- mixed: bfloat16 [32, 2048], P(('grp', 'ep')), parts along dimension 0
- new_latent: bfloat16 [32, 512], P(('grp', 'ep')), parts along dimension 0
- new_rope: bfloat16 [32, 32], P(('grp', 'ep')), parts along dimension 0
There are 2 independent parts, one for each index of `grp`. A program takes and returns all parts, laid end to end along the dimension named above; an argument that names none is the same for every part. Nothing has to cross between parts.
Inputs may be any that keep to these rules, and one draw needn't show every extreme that they name: `routes`: each row names 2 different experts; over one part's 16 tokens no expert is named by more than 4 rows, a bound that some block reaches. `lengths`: some sequence has all 3072 positions filled.
All inputs are finite; a program needn't handle non-finite values.
Results may differ from a plain program's by a relative error of at most 0.013.
Values may be sent and summed in bfloat16 or wider, within the bound.
No kernel may reach another device: no remote copies, remote signals or barrier semaphores. Data moves between devices by JAX's collectives and lax.ppermute only.
A program may use at most 64 MiB of HBM per device.

v0:
```python
import jax
import jax.numpy as jnp
from jax import lax
from jax.sharding import PartitionSpec as P

D = 2048
HEADS = 16
NOPE = 64
ROPE = 32
VDIM = 64
LATENT = 512
CAP = 4


EPS = 1e-06
THETA = 10000.0


def rms_scale(values, gain):
    return values * lax.rsqrt(jnp.mean(values * values, axis=-1, keepdims=True) + EPS) * gain


def rope_tables(positions, width):
    inverse = THETA ** (-jnp.arange(0, width, 2).astype(jnp.float32) / width)
    angle = positions.astype(jnp.float32)[:, None] * inverse[None, :]
    return (jnp.cos(angle), jnp.sin(angle))


def apply_rope(values, cosine, sine):
    half = values.shape[-1] // 2
    first, second = (values[..., :half], values[..., half:])
    return jnp.concatenate(
        [first * cosine - second * sine, second * cosine + first * sine], axis=-1
    )


def body(
    tokens,
    cache_latent,
    cache_rope,
    lengths,
    w_query,
    w_latent,
    w_rope,
    w_absorb,
    w_value,
    w_output,
    gain_attn,
    gain_latent,
    gain_moe,
    routes,
    route_scores,
    w_gate,
    w_up,
    w_down,
):
    local_seqs = tokens.shape[0]
    devices = lax.axis_size("ep")
    q_width = w_query.shape[1]
    lat_width = w_latent.shape[1]
    normed = rms_scale(tokens.astype(jnp.float32), gain_attn).astype(jnp.bfloat16)
    feature_rows = lax.all_to_all(normed, "ep", split_axis=1, concat_axis=0, tiled=True)
    stacked = jnp.concatenate([w_query, w_latent, w_rope], axis=1)
    rows = feature_rows
    summed = lax.psum_scatter(
        jnp.dot(rows, stacked, preferred_element_type=jnp.float32),
        "ep",
        scatter_dimension=0,
        tiled=True,
    )
    query = summed[:, :q_width].astype(jnp.bfloat16)
    latent_raw = summed[:, q_width : q_width + lat_width].astype(jnp.bfloat16)
    rope_raw = summed[:, q_width + lat_width :].astype(jnp.bfloat16)
    new_latent = rms_scale(latent_raw.astype(jnp.float32), gain_latent).astype(jnp.bfloat16)
    cosine, sine = rope_tables(lengths, ROPE)
    new_rope = apply_rope(rope_raw.astype(jnp.float32), cosine, sine).astype(jnp.bfloat16)
    heads_view = query.reshape(local_seqs, HEADS, NOPE + ROPE)
    q_nope = heads_view[:, :, :NOPE]
    q_pe = apply_rope(
        heads_view[:, :, NOPE:].astype(jnp.float32), cosine[:, None, :], sine[:, None, :]
    ).astype(jnp.bfloat16)
    q_abs = jnp.einsum(
        "shn,chn->shc",
        q_nope,
        w_absorb.reshape(LATENT, HEADS, NOPE),
        preferred_element_type=jnp.float32,
    ).astype(jnp.bfloat16)
    scale = (NOPE + ROPE) ** (-0.5)
    past = (
        jnp.einsum("shc,skc->shk", q_abs, cache_latent, preferred_element_type=jnp.float32)
        + jnp.einsum("shr,srk->shk", q_pe, cache_rope, preferred_element_type=jnp.float32)
    ) * scale
    fresh = (
        jnp.einsum("shc,sc->sh", q_abs, new_latent, preferred_element_type=jnp.float32)
        + jnp.einsum("shr,sr->sh", q_pe, new_rope, preferred_element_type=jnp.float32)
    ) * scale
    valid = jnp.arange(cache_latent.shape[1])[None, None, :] < lengths[:, None, None]
    top = jnp.maximum(jnp.max(jnp.where(valid, past, -jnp.inf), axis=-1), fresh)
    e_past = jnp.where(valid, jnp.exp(past - top[:, :, None]), 0.0)
    e_new = jnp.exp(fresh - top)
    total = jnp.sum(e_past, axis=-1) + e_new
    p_past = (e_past / total[:, :, None]).astype(jnp.bfloat16)
    p_new = (e_new / total).astype(jnp.bfloat16)
    attended = (
        jnp.einsum("shk,skc->shc", p_past, cache_latent, preferred_element_type=jnp.float32)
        + p_new.astype(jnp.float32)[:, :, None] * new_latent.astype(jnp.float32)[:, None, :]
    ).astype(jnp.bfloat16)
    values = jnp.einsum(
        "shc,chv->shv",
        attended,
        w_value.reshape(LATENT, HEADS, VDIM),
        preferred_element_type=jnp.float32,
    ).astype(jnp.bfloat16)
    values = values.reshape(local_seqs, HEADS * VDIM)
    head_rows = lax.all_to_all(values, "ep", split_axis=1, concat_axis=0, tiled=True)
    rows = head_rows
    attn_out = lax.psum_scatter(
        jnp.dot(rows, w_output, preferred_element_type=jnp.float32),
        "ep",
        scatter_dimension=0,
        tiled=True,
    )
    resid = (tokens.astype(jnp.float32) + attn_out).astype(jnp.bfloat16)
    moe_in = rms_scale(resid.astype(jnp.float32), gain_moe).astype(jnp.bfloat16)
    route_weight = route_scores / jnp.sum(route_scores, axis=-1, keepdims=True)
    slots = jnp.arange(CAP).astype(jnp.float32)
    expert_ids = jnp.arange(devices)
    hits = routes[:, :, None] == expert_ids[None, None, :]
    chosen = jnp.any(hits, axis=1)
    outgoing = jnp.where(chosen.T[:, :, None], moe_in[None, :, :], jnp.zeros((), jnp.bfloat16))
    flags_out = chosen.T.astype(jnp.bfloat16)
    arrived, arrived_flags = (
        lax.all_to_all(outgoing, "ep", split_axis=0, concat_axis=0, tiled=True),
        lax.all_to_all(flags_out, "ep", split_axis=0, concat_axis=0, tiled=True),
    )
    flat_rows = arrived.reshape(devices * local_seqs, D)
    flag = arrived_flags.reshape(-1).astype(jnp.float32)
    rank = jnp.cumsum(flag) - 1.0
    picker = ((rank[None, :] == slots[:, None]) & (flag[None, :] > 0.5)).astype(jnp.bfloat16)
    packed = jnp.dot(picker, flat_rows, preferred_element_type=jnp.float32).astype(jnp.bfloat16)
    gate = jnp.dot(packed, w_gate[0], preferred_element_type=jnp.float32)
    upper = jnp.dot(packed, w_up[0], preferred_element_type=jnp.float32)
    hidden = (jax.nn.silu(gate) * upper).astype(jnp.bfloat16)
    result = jnp.dot(hidden, w_down[0], preferred_element_type=jnp.float32).astype(jnp.bfloat16)
    spread = (
        jnp.dot(picker.T, result, preferred_element_type=jnp.float32)
        .astype(jnp.bfloat16)
        .reshape(devices, local_seqs, D)
    )
    answers = lax.all_to_all(spread, "ep", split_axis=0, concat_axis=0, tiled=True)
    weight_table = jnp.sum(hits.astype(jnp.float32) * route_weight[:, :, None], axis=1)
    moe_sum = jnp.einsum("sn,nsd->sd", weight_table, answers.astype(jnp.float32))
    mixed = (resid.astype(jnp.float32) + moe_sum).astype(jnp.bfloat16)
    return (mixed, new_latent, new_rope)


def solution(mesh):
    placed = (
        P(("grp", "ep"), None),
        P(("grp", "ep"), None, None),
        P(("grp", "ep"), None, None),
        P(("grp", "ep")),
        P("ep", None),
        P("ep", None),
        P("ep", None),
        P(),
        P(),
        P("ep", None),
        P(),
        P(),
        P(),
        P(("grp", "ep"), None),
        P(("grp", "ep"), None),
        P("ep", None, None),
        P("ep", None, None),
        P("ep", None, None),
    )
    return jax.shard_map(
        body,
        mesh=mesh,
        in_specs=placed,
        out_specs=(P(("grp", "ep"), None), P(("grp", "ep"), None), P(("grp", "ep"), None)),
        check_vma=False,
    )
```

profile of v0, /device:TPU:0, one launch (start us, length us, event | category | flops | bytes accessed | tf_op | source)
XLA Modules:
  0.0 251.2 jit_solution(14242424086697697236)
XLA Ops:
  7.2 1.5 multiply_reduce_fusion.1
  9.3 1.3 convert_bitcast_fusion
  10.7 7.4 %all-to-all-start = ((bf16[1,16,128]{2,0,1:T(2,128)(2,1)}), bf16[1,16,128]{2,0,1:T(2,128)(2,1)S(1)}, u32[]{:S(2)}, u32[]{:S(2)}) async-start(bf16[1,16,128]{2,0,1:T(2,128)(2,1)} %convert_bitcast_fusion), calls=%async_computation | async-start | bytes 16384 | tf_op jit(solution)/shard_map/all_to_all | solution.py:62
  18.8 0.7 fusion.67
  19.5 0.5 convert_bitcast_fusion.2
  20.0 0.6 fusion.77
  20.6 0.8 copy.40
  21.5 2.3 copy.41
  23.8 2.3 copy.42
  26.1 0.6 dynamic-slice
  26.7 0.7 reduce_sum.57
  27.3 1.3 fusion.30
  28.6 63.5 %all-reduce.6 = bf16[16,2080]{1,0:T(8,128)(2,1)S(1)} all-reduce(f32[16,2080]{1,0:T(8,128)S(1)} %fusion.30), channel_id=2, replica_groups=mesh['grp'=2,'ep'=16] {'ep'}, use_global_device_ids=true, to_apply=%region_1.0.clone | all-reduce | flops 33280 | bytes 199680
  92.1 0.7 dynamic-slice_convert_fusion
  93.0 0.6 multiply_reduce_fusion.2
  94.4 0.7 fusion.86
  95.1 1.5 fusion.51
  96.7 0.7 fusion.56
  97.4 0.2 fusion.36
  97.6 1.0 select_reduce_fusion
  98.9 0.2 fusion.38
  99.2 0.6 fusion.17
  99.9 0.4 fusion.47
  100.3 0.6 copy.43
  100.9 3.5 %all-to-all-start.1 = ((bf16[1,16,64]{2,0,1:T(2,128)(2,1)}), bf16[1,16,64]{2,0,1:T(2,128)(2,1)S(1)}, u32[]{:S(2)}, u32[]{:S(2)}) async-start(bf16[1,16,64]{2,0,1:T(2,128)(2,1)} %copy.43), calls=%async_computation.1 | async-start | bytes 16384 | tf_op jit(solution)/shard_map/all_to_all | solution.py:115
  104.4 0.6 divide_bitcast_fusion
  105.0 0.7 copy.44
  105.7 5.0 %all-to-all-done.1 = bf16[1,16,64]{2,0,1:T(2,128)(2,1)S(1)} async-done(((bf16[1,16,64]{2,0,1:T(2,128)(2,1)}), bf16[1,16,64]{2,0,1:T(2,128)(2,1)S(1)}, u32[]{:S(2)}, u32[]{:S(2)}) %all-to-all-start.1) | async-done | bytes 2080 | tf_op jit(solution)/shard_map/all_to_all | solution.py:115
  110.7 3.5 %all-to-all-start.2 = ((bf16[16,1,1]{2,1,0:T(2,128)(2,1)}), bf16[16,1,1]{2,1,0:T(2,128)(2,1)S(1)}, u32[]{:S(2)}, u32[]{:S(2)}) async-start(bf16[16,1,1]{2,1,0:T(2,128)(2,1)} %copy.44), calls=%async_computation.2 | async-start | bytes 16384 | tf_op jit(solution)/shard_map/all_to_all | solution.py:134
  114.3 0.8 fusion.58
  115.1 5.5 %all-to-all-done.2 = bf16[16,1,1]{2,1,0:T(2,128)(2,1)S(1)} async-done(((bf16[16,1,1]{2,1,0:T(2,128)(2,1)}), bf16[16,1,1]{2,1,0:T(2,128)(2,1)S(1)}, u32[]{:S(2)}, u32[]{:S(2)}) %all-to-all-start.2) | async-done | bytes 64 | tf_op jit(solution)/shard_map/all_to_all | solution.py:134
  120.6 87.4 %all-reduce.5.cloned.1.call-done = f32[16,2048]{1,0:T(8,128)} async-done(((f32[16,2048]{1,0:T(8,128)}), f32[16,2048]{1,0:T(8,128)}) %all-reduce.5.cloned.1.call-update) | async-done | bytes 131088
  208.0 2.1 multiply_reduce_fusion
  211.1 0.5 broadcast.345
  211.6 1.0 reduce.20
  212.6 0.7 reshape.512
  213.2 6.3 %all-to-all-start.3 = ((bf16[16,2,1024]{2,1,0:T(2,128)(2,1)}), bf16[16,2,1024]{2,1,0:T(2,128)(2,1)S(1)}, u32[]{:S(2)}, u32[]{:S(2)}) async-start(bf16[16,2,1024]{2,1,0:T(2,128)(2,1)} %reshape.512), calls=%async_computation.3 | async-start | bytes 131072 | tf_op jit(solution)/shard_map/all_to_all | solution.py:133
  219.6 0.4 compare_reduce_fusion
  220.0 6.4 %all-to-all-done.3 = bf16[16,2,1024]{2,1,0:T(2,128)(2,1)S(1)} async-done(((bf16[16,2,1024]{2,1,0:T(2,128)(2,1)}), bf16[16,2,1024]{2,1,0:T(2,128)(2,1)S(1)}, u32[]{:S(2)}, u32[]{:S(2)}) %all-to-all-start.3) | async-done | bytes 65568 | tf_op jit(solution)/shard_map/all_to_all | solution.py:133
  226.7 2.0 fusion.9
  228.6 3.0 %convolution_convert_fusion.1 = bf16[4,2048]{1,0:T(4,128)(2,1)S(1)} fusion(bf16[1,512,2048]{2,1,0:T(8,128)(2,1)} %param.35, bf16[4,2048]{1,0:T(4,128)(2,1)S(1)} %convolution_convert_fusion.2, bf16[1,2048,512]{2,1,0:T(8,128)(2,1)} %param.34, f32[4,512]{1,0:T(4,128)S(1)} %fusion.9), kind=kOutput, calls=%fused_computation.7 | convolution fusion | flops 16797696 | bytes 4235264 | tf_op jit(solution)/shard_map/dot_general | solution.py:144
  231.6 0.3 fusion.4
  231.9 0.7 reduce.21
  232.6 0.7 reshape.514
  233.2 3.5 %all-to-all-start.4 = ((bf16[16,2,1024]{2,1,0:T(2,128)(2,1)}), bf16[16,2,1024]{2,1,0:T(2,128)(2,1)S(1)}, u32[]{:S(2)}, u32[]{:S(2)}) async-start(bf16[16,2,1024]{2,1,0:T(2,128)(2,1)} %reshape.514), calls=%async_computation.4 | async-start | bytes 131072 | tf_op jit(solution)/shard_map/all_to_all | solution.py:150
  236.8 0.6 pad_maximum_fusion.3
  237.4 6.2 %all-to-all-done.4 = bf16[16,2,1024]{2,1,0:T(2,128)(2,1)S(1)} async-done(((bf16[16,2,1024]{2,1,0:T(2,128)(2,1)}), bf16[16,2,1024]{2,1,0:T(2,128)(2,1)S(1)}, u32[]{:S(2)}, u32[]{:S(2)}) %all-to-all-start.4) | async-done | bytes 65568 | tf_op jit(solution)/shard_map/all_to_all | solution.py:150
  243.6 0.8 fusion.5
  (53 shorter events, 1.6 us)
Async XLA Ops:
  7.2 90.5 %copy-start = (bf16[1,3072,512]{2,1,0:T(8,128)(2,1)S(1)}, bf16[1,3072,512]{2,1,0:T(8,128)(2,1)}, u32[]{:S(2)}) copy-start(bf16[1,3072,512]{2,1,0:T(8,128)(2,1)} %param.19) | copy-start | bytes 9437188
  10.7 16.7 %all-to-all-start = ((bf16[1,16,128]{2,0,1:T(2,128)(2,1)}), bf16[1,16,128]{2,0,1:T(2,128)(2,1)S(1)}, u32[]{:S(2)}, u32[]{:S(2)}) async-start(bf16[1,16,128]{2,0,1:T(2,128)(2,1)} %convert_bitcast_fusion), calls=%async_computation | async-start | bytes 16384 | tf_op jit(solution)/shard_map/all_to_all | solution.py:62
  19.5 6.6 %copy-start.7 = (pred[16]{0:T(512)(128)(4,1)}, pred[16]{0:T(512)(128)(4,1)S(1)}, u32[]{:S(2)}) copy-start(pred[16]{0:T(512)(128)(4,1)S(1)} %fusion.67) | copy-start | bytes 52
  21.4 4.7 %copy-start.13 = (u32[32]{0:T(128)S(1)}, u32[32]{0:T(128)}, u32[]{:S(2)}) copy-start(u32[32]{0:T(128)} %constant.56) | copy-start | bytes 388
  21.4 5.2 %copy-start.10 = (f32[1,2]{1,0:T(1,128)S(1)}, f32[1,2]{1,0:T(1,128)}, u32[]{:S(2)}) copy-start(f32[1,2]{1,0:T(1,128)} %param.32) | copy-start | bytes 28
  23.8 73.6 %copy-start.3 = (bf16[1,32,3072]{2,1,0:T(8,128)(2,1)S(1)}, bf16[1,32,3072]{2,1,0:T(8,128)(2,1)}, u32[]{:S(2)}) copy-start(bf16[1,32,3072]{2,1,0:T(8,128)(2,1)} %param.20) | copy-start | bytes 589828
  95.1 3.6 %copy-start.6 = (bf16[1,512]{1,0:T(2,128)(2,1)}, bf16[1,512]{1,0:T(2,128)(2,1)S(1)}, u32[]{:S(2)}) copy-start(bf16[1,512]{1,0:T(2,128)(2,1)S(1)} %get-tuple-element.6) | copy-start | bytes 3076
  98.7 1.2 copy-start.1
  99.1 5.3 %copy-start.11 = (f32[1,2]{1,0:T(1,128)S(1)}, f32[1,2]{1,0:T(1,128)}, u32[]{:S(2)}) copy-start(f32[1,2]{1,0:T(1,128)} %param.32) | copy-start | bytes 28
  99.1 5.9 %copy-start.9 = (bf16[16,1,1]{0,2,1:T(2,128)(2,1)S(1)}, bf16[16,1,1]{0,2,1:T(2,128)(2,1)}, u32[]{:S(2)}) copy-start(bf16[16,1,1]{0,2,1:T(2,128)(2,1)} %convert_bitcast_fusion.2) | copy-start | bytes 100
  99.1 15.1 %copy-start.2 = (bf16[64,2048]{1,0:T(8,128)(2,1)S(1)}, bf16[64,2048]{1,0:T(8,128)(2,1)}, u32[]{:S(2)}) copy-start(bf16[64,2048]{1,0:T(8,128)(2,1)} %param.27) | copy-start | bytes 786436
  99.2 108.9 %copy-start.4 = (bf16[1,2048]{1,0:T(2,128)(2,1)S(1)}, bf16[1,2048]{1,0:T(2,128)(2,1)}, u32[]{:S(2)}) copy-start(bf16[1,2048]{1,0:T(2,128)(2,1)} %param.18) | copy-start | bytes 12292
  99.2 111.7 %copy-start.5 = (f32[2048]{0:T(1024)S(1)}, f32[2048]{0:T(1024)}, u32[]{:S(2)}) copy-start(f32[2048]{0:T(1024)} %param.30) | copy-start | bytes 24580
  99.2 111.7 %copy-start.8 = (pred[16]{0:T(512)(128)(4,1)S(1)}, pred[16]{0:T(512)(128)(4,1)}, u32[]{:S(2)}) copy-start(pred[16]{0:T(512)(128)(4,1)} %copy-done.7) | copy-start | bytes 52
  100.9 9.8 %all-to-all-start.1 = ((bf16[1,16,64]{2,0,1:T(2,128)(2,1)}), bf16[1,16,64]{2,0,1:T(2,128)(2,1)S(1)}, u32[]{:S(2)}, u32[]{:S(2)}) async-start(bf16[1,16,64]{2,0,1:T(2,128)(2,1)} %copy.43), calls=%async_computation.1 | async-start | bytes 16384 | tf_op jit(solution)/shard_map/all_to_all | solution.py:115
  110.7 9.9 %all-to-all-start.2 = ((bf16[16,1,1]{2,1,0:T(2,128)(2,1)}), bf16[16,1,1]{2,1,0:T(2,128)(2,1)S(1)}, u32[]{:S(2)}, u32[]{:S(2)}) async-start(bf16[16,1,1]{2,1,0:T(2,128)(2,1)} %copy.44), calls=%async_computation.2 | async-start | bytes 16384 | tf_op jit(solution)/shard_map/all_to_all | solution.py:134
  114.2 93.8 %all-reduce.5.cloned.1.call-start = ((), (), s32[]{:S(2)}) async-start(), calls=%async_computation.5 | async-start | bytes 262144
  213.2 13.2 %all-to-all-start.3 = ((bf16[16,2,1024]{2,1,0:T(2,128)(2,1)}), bf16[16,2,1024]{2,1,0:T(2,128)(2,1)S(1)}, u32[]{:S(2)}, u32[]{:S(2)}) async-start(bf16[16,2,1024]{2,1,0:T(2,128)(2,1)} %reshape.512), calls=%async_computation.3 | async-start | bytes 131072 | tf_op jit(solution)/shard_map/all_to_all | solution.py:133
  228.6 8.1 %copy-start.12 = (s32[1,2]{1,0:T(1,128)S(1)}, s32[1,2]{1,0:T(1,128)}, u32[]{:S(2)}) copy-start(s32[1,2]{1,0:T(1,128)} %param.31) | copy-start | bytes 28
  233.2 10.4 %all-to-all-start.4 = ((bf16[16,2,1024]{2,1,0:T(2,128)(2,1)}), bf16[16,2,1024]{2,1,0:T(2,128)(2,1)S(1)}, u32[]{:S(2)}, u32[]{:S(2)}) async-start(bf16[16,2,1024]{2,1,0:T(2,128)(2,1)} %reshape.514), calls=%async_computation.4 | async-start | bytes 131072 | tf_op jit(solution)/shard_map/all_to_all | solution.py:150
Sparse Core Ops, SparseCore 0:
  118.5 89.5 all-reduce.4
where the time goes:
time: 252 us; the launch traced here: 251 us
  waiting for transfers between devices  110 us (44%)
  blocking collectives  63.5 us (25%)
  starting transfers between devices  24.2 us (10%)
  between operations  17.1 us (7%)
  other arithmetic  13.6 us (5%)
  matrix products  12.2 us (5%)
  local copies, waits for them, and re-layouts  10.3 us (4%)
    unnamed x2, waiting for transfers between devices  87.4 us
    unnamed x1, blocking collectives  63.5 us
    unnamed x36, local copies, waits for them, and re-layouts  7.66 us
    all_to_all x1, starting transfers between devices, body(): lax.all_to_all(normed, 'ep', split_axis=1, concat_axis=0, tiled=True)  7.41 us
    all_to_all x1, waiting for transfers between devices, body(): lax.all_to_all(outgoing, 'ep', split_axis=0, concat_axis=0, tiled=True)  6.39 us
    all_to_all x1, starting transfers between devices, body(): lax.all_to_all(outgoing, 'ep', split_axis=0, concat_axis=0, tiled=True)  6.26 us
    all_to_all x1, waiting for transfers between devices, body(): lax.all_to_all(spread, 'ep', split_axis=0, concat_axis=0, tiled=True)  6.17 us
    all_to_all x1, waiting for transfers between devices, body(): lax.all_to_all(flags_out, 'ep', split_axis=0, concat_axis=0, tiled=True)  5.49 us
  transfers between devices with their start and end apart: 6, of which 5 were waited for; matrix products, arithmetic and copies ran while one was open for 5% of the time, Pallas kernels for 0%

commit v1 on v0

v1 whole, which is shorter than its diff:
```python
import jax
import jax.numpy as jnp
from jax import lax
from jax.sharding import PartitionSpec as P

D = 2048
HEADS = 16
NOPE = 64
ROPE = 32
VDIM = 64
LATENT = 512
CAP = 4
LANES = 128


EPS = 1e-06
THETA = 10000.0


def rms_scale(values, gain):
    return values * lax.rsqrt(jnp.mean(values * values, axis=-1, keepdims=True) + EPS) * gain


def rope_tables(positions, width):
    inverse = THETA ** (-jnp.arange(0, width, 2).astype(jnp.float32) / width)
    angle = positions.astype(jnp.float32)[:, None] * inverse[None, :]
    return (jnp.cos(angle), jnp.sin(angle))


def apply_rope(values, cosine, sine):
    half = values.shape[-1] // 2
    first, second = (values[..., :half], values[..., half:])
    return jnp.concatenate(
        [first * cosine - second * sine, second * cosine + first * sine], axis=-1
    )


def body(
    tokens,
    cache_latent,
    cache_rope,
    lengths,
    w_query,
    w_latent,
    w_rope,
    w_absorb,
    w_value,
    w_output,
    gain_attn,
    gain_latent,
    gain_moe,
    routes,
    route_scores,
    w_gate,
    w_up,
    w_down,
):
    local_seqs, width = tokens.shape
    devices = lax.axis_size("ep")
    me = lax.axis_index("ep")
    total_rows = devices * local_seqs
    block = w_query.shape[0]
    heads = HEADS
    q_width = w_query.shape[1]
    lat_width = w_latent.shape[1]
    bf16, f32 = jnp.bfloat16, jnp.float32

    top_k = routes.shape[1]
    tagged = jnp.concatenate(
        [tokens, routes.astype(bf16), jnp.zeros((local_seqs, LANES - top_k), bf16)], axis=1
    )
    tagged = jnp.broadcast_to(tagged[None], (devices,) + tagged.shape).reshape(total_rows, -1)
    gathered = lax.all_to_all(tagged, "ep", split_axis=0, concat_axis=0, tiled=True)
    all_tokens = gathered[:, :width]
    all_routes = gathered[:, width : width + top_k].astype(jnp.int32)

    all32 = all_tokens.astype(f32)
    scale_rows = lax.rsqrt(jnp.mean(all32 * all32, axis=-1, keepdims=True) + EPS)
    my_cols = lax.dynamic_slice_in_dim(all_tokens, me * block, block, axis=1).astype(f32)
    my_gain = lax.dynamic_slice_in_dim(gain_attn, me * block, block, axis=0)
    rows = (my_cols * scale_rows * my_gain).astype(bf16)
    partial = jnp.concatenate(
        [
            jnp.dot(rows, w_query, preferred_element_type=f32),
            jnp.dot(rows, w_latent, preferred_element_type=f32),
            jnp.dot(rows, w_rope, preferred_element_type=f32),
        ],
        axis=1,
    )
    partial = lax.all_to_all(partial, "ep", split_axis=0, concat_axis=0, tiled=True)
    summed = jnp.sum(partial.reshape(devices, local_seqs, -1), axis=0)

    token_ids = jnp.arange(total_rows)
    expert_ids = jnp.arange(devices)
    chosen = jnp.any(all_routes[:, :, None] == expert_ids[None, None, :], axis=1)
    before = (token_ids[None, :] < token_ids[:, None]).astype(bf16)
    rank = jnp.dot(before, chosen.astype(bf16), preferred_element_type=f32)
    ranked = jnp.where(chosen, rank, -1.0)
    slots = jnp.arange(CAP).astype(f32)
    routed = ranked.T[:, None, :] == slots[None, :, None]
    owned = (
        token_ids[None, None, :]
        == (expert_ids[:, None] * local_seqs + jnp.arange(local_seqs)[None, :])[:, :, None]
    )
    sel = jnp.concatenate([owned, routed], axis=1).astype(bf16)
    per = local_seqs + CAP
    sel_mine = lax.dynamic_slice_in_dim(sel, me, 1, axis=0)[0]
    tokens_mine = jnp.dot(sel_mine, all_tokens, preferred_element_type=f32)
    picker = sel_mine[local_seqs:]
    hits = routes[:, :, None] == expert_ids[None, None, :]
    route_weight = route_scores / jnp.sum(route_scores, axis=-1, keepdims=True)
    weight_table = jnp.sum(hits.astype(f32) * route_weight[:, :, None], axis=1)

    query = summed[:, :q_width].astype(bf16)
    latent_raw = summed[:, q_width : q_width + lat_width].astype(bf16)
    rope_raw = summed[:, q_width + lat_width :].astype(bf16)
    new_latent = rms_scale(latent_raw.astype(f32), gain_latent).astype(bf16)
    cosine, sine = rope_tables(lengths, ROPE)
    new_rope = apply_rope(rope_raw.astype(f32), cosine, sine).astype(bf16)
    heads_view = query.reshape(local_seqs, heads, NOPE + ROPE)
    q_nope = heads_view[:, :, :NOPE]
    q_pe = apply_rope(
        heads_view[:, :, NOPE:].astype(f32), cosine[:, None, :], sine[:, None, :]
    ).astype(bf16)
    head_ids = jnp.arange(heads)
    own_key = (jnp.arange(heads * NOPE) // NOPE)[None, None, :] == head_ids[None, :, None]
    spread_q = jnp.where(own_key, jnp.tile(q_nope, (1, 1, heads)), jnp.zeros((), bf16))
    q_abs = jnp.einsum("shm,cm->shc", spread_q, w_absorb, preferred_element_type=f32).astype(bf16)
    scale = (NOPE + ROPE) ** (-0.5)
    past = (
        jnp.einsum("shc,skc->shk", q_abs, cache_latent, preferred_element_type=f32)
        + jnp.einsum("shr,srk->shk", q_pe, cache_rope, preferred_element_type=f32)
    ) * scale
    fresh = (
        jnp.einsum("shc,sc->sh", q_abs, new_latent, preferred_element_type=f32)
        + jnp.einsum("shr,sr->sh", q_pe, new_rope, preferred_element_type=f32)
    ) * scale
    valid = jnp.arange(cache_latent.shape[1])[None, None, :] < lengths[:, None, None]
    top = jnp.maximum(jnp.max(jnp.where(valid, past, -jnp.inf), axis=-1), fresh)
    e_past = jnp.where(valid, jnp.exp(past - top[:, :, None]), 0.0)
    e_new = jnp.exp(fresh - top)
    total = jnp.sum(e_past, axis=-1) + e_new
    p_past = (e_past / total[:, :, None]).astype(bf16)
    p_new = (e_new / total).astype(bf16)
    attended = (
        jnp.einsum("shk,skc->shc", p_past, cache_latent, preferred_element_type=f32)
        + p_new.astype(f32)[:, :, None] * new_latent.astype(f32)[:, None, :]
    ).astype(bf16)
    all_heads = jnp.einsum("shc,cm->shm", attended, w_value, preferred_element_type=f32)
    own_value = (jnp.arange(heads * VDIM) // VDIM)[None, None, :] == head_ids[None, :, None]
    values = jnp.sum(jnp.where(own_value, all_heads, 0.0), axis=1).astype(bf16)

    head_rows = lax.all_to_all(values, "ep", split_axis=1, concat_axis=0, tiled=True)
    picked = jnp.dot(sel.reshape(devices * per, total_rows), head_rows,
                     preferred_element_type=f32).astype(bf16)
    out_part = jnp.dot(picked, w_output, preferred_element_type=f32).astype(bf16)
    out_part = lax.all_to_all(
        out_part.reshape(devices, per, width), "ep", split_axis=0, concat_axis=0, tiled=True
    )
    attn_out = jnp.sum(out_part.astype(f32), axis=0)
    resid = (tokens_mine + attn_out).astype(bf16)
    moe_in = rms_scale(resid.astype(f32), gain_moe).astype(bf16)
    packed = moe_in[local_seqs:]
    gate = jnp.dot(packed, w_gate[0], preferred_element_type=f32)
    upper = jnp.dot(packed, w_up[0], preferred_element_type=f32)
    hidden = (jax.nn.silu(gate) * upper).astype(bf16)
    result = jnp.dot(hidden, w_down[0], preferred_element_type=f32).astype(bf16)
    spread = jnp.dot(picker.T, result, preferred_element_type=f32).astype(bf16)
    answers = lax.all_to_all(spread, "ep", split_axis=0, concat_axis=0, tiled=True)
    answers = answers.reshape(devices, local_seqs, width)
    moe_sum = jnp.einsum("sn,nsd->sd", weight_table, answers.astype(f32))
    mixed = (resid[:local_seqs].astype(f32) + moe_sum).astype(bf16)
    return (mixed, new_latent, new_rope)


def solution(mesh):
    placed = (
        P(("grp", "ep"), None),
        P(("grp", "ep"), None, None),
        P(("grp", "ep"), None, None),
        P(("grp", "ep")),
        P("ep", None),
        P("ep", None),
        P("ep", None),
        P(),
        P(),
        P("ep", None),
        P(),
        P(),
        P(),
        P(("grp", "ep"), None),
        P(("grp", "ep"), None),
        P("ep", None, None),
        P("ep", None, None),
        P("ep", None, None),
    )
    return jax.shard_map(
        body,
        mesh=mesh,
        in_specs=placed,
        out_specs=(P(("grp", "ep"), None), P(("grp", "ep"), None), P(("grp", "ep"), None)),
        check_vma=False,
    )
```

time: 252 us -> 96.6 us (0.38)
  waiting for transfers between devices: 110 us -> 37.3 us
  blocking collectives: 63.5 us -> 0 us
  between operations: 17.1 us -> 2.32 us
  other arithmetic: 13.6 us -> 8.09 us
  matrix products: 12.2 us -> 17.1 us
  local copies, waits for them, and re-layouts: 10.3 us -> 7.48 us
    unnamed x2 -> x0, waiting for transfers between devices: 87.4 us -> none
    unnamed x1 -> x0, blocking collectives: 63.5 us -> none
    all_to_all x3, waiting for transfers between devices: 11.9 us -> 25.5 us  [the longest x1 12.3 us: body(): lax.all_to_all(out_part.reshape(devices, per, width), 'ep', split_axis=0,...]
    unnamed x36 -> x28, local copies, waits for them, and re-layouts: 7.66 us -> 1.74 us
    dot_general x14 -> x16, matrix products: 12.2 us -> 17.1 us  [the longest x1 2.99 us: body(): result = jnp.dot(hidden, w_down[0], preferred_element_type=f32).astype(bf16)]
    reduce_sum x3 -> x2, other arithmetic: 4.19 us -> 0.74 us  [rms_scale(): jnp.mean(values * values, axis=-1, keepdims=True) + EPS]
  transfers between devices with their start and end apart: 6 -> 5, of which waited for: 5 -> 5; matrix products, arithmetic and copies ran while one was open for 5% -> 5% of each run, Pallas kernels for 0% -> 0%
where the time goes in v1:
time: 96.6 us; the launch traced here: 95.6 us
  waiting for transfers between devices  37.3 us (39%)
  starting transfers between devices  23.4 us (24%)
  matrix products  17.1 us (18%)
  other arithmetic  8.09 us (8%)
  local copies, waits for them, and re-layouts  7.48 us (8%)
  between operations  2.32 us (2%)
    all_to_all x1, waiting for transfers between devices, body(): lax.all_to_all(out_part.reshape(devices, per, width), 'ep', split_axis=0,...  12.3 us
    all_to_all x1, waiting for transfers between devices, body(): lax.all_to_all(partial, 'ep', split_axis=0, concat_axis=0, tiled=True)  7.73 us
    all_to_all x1, starting transfers between devices, body(): lax.all_to_all(tagged, 'ep', split_axis=0, concat_axis=0, tiled=True)  7.41 us
    all_to_all x1, waiting for transfers between devices, body(): lax.all_to_all(spread, 'ep', split_axis=0, concat_axis=0, tiled=True)  6.2 us
    all_to_all x1, waiting for transfers between devices, body(): lax.all_to_all(values, 'ep', split_axis=1, concat_axis=0, tiled=True)  5.55 us
    all_to_all x1, waiting for transfers between devices, body(): lax.all_to_all(tagged, 'ep', split_axis=0, concat_axis=0, tiled=True)  5.46 us
    all_to_all x1, starting transfers between devices, body(): lax.all_to_all(out_part.reshape(devices, per, width), 'ep', split_axis=0,...  4.37 us
    all_to_all x1, starting transfers between devices, body(): lax.all_to_all(spread, 'ep', split_axis=0, concat_axis=0, tiled=True)  4.08 us
  transfers between devices with their start and end apart: 5, of which 5 were waited for; matrix products, arithmetic and copies ran while one was open for 5% of the time, Pallas kernels for 0%

profile of v1, /device:TPU:0, one launch (start us, length us, event | category | flops | bytes accessed | tf_op | source)
XLA Modules:
  0.0 95.6 jit_solution(15410883736584302631)
XLA Ops:
  0.7 0.8 convert_element_type.152
  1.5 0.9 concatenate.43
  2.5 0.5 broadcast.358
  3.0 1.0 %reduce.17 = bf16[16,2176]{1,0:T(8,128)(2,1)S(1)} reduce(bf16[16,1,2176]{2,1,0:T(2,128)(2,1)S(1)} %reshape.416, bf16[]{:T(256)} %broadcast.358), dimensions={1}, to_apply=%reshape.416.reduce_sub_computation | reduce | bytes 139266 | tf_op jit(solution)/shard_map/reshape | solution.py:72
  4.1 0.8 reshape.435
  4.8 7.4 %all-to-all-start = ((bf16[16,2,1088]{2,1,0:T(2,128)(2,1)}), bf16[16,2,1088]{2,1,0:T(2,128)(2,1)S(1)}, u32[]{:S(2)}, u32[]{:S(2)}) async-start(bf16[16,2,1088]{2,1,0:T(2,128)(2,1)} %reshape.435), calls=%async_computation | async-start | bytes 147456 | tf_op jit(solution)/shard_map/all_to_all | solution.py:73
  13.0 0.8 dynamic_slice.11
  13.8 5.5 %all-to-all-done = bf16[16,2,1088]{2,1,0:T(2,128)(2,1)S(1)} async-done(((bf16[16,2,1088]{2,1,0:T(2,128)(2,1)}), bf16[16,2,1088]{2,1,0:T(2,128)(2,1)S(1)}, u32[]{:S(2)}, u32[]{:S(2)}) %all-to-all-start) | async-done | bytes 69664 | tf_op jit(solution)/shard_map/all_to_all | solution.py:73
  19.4 0.1 multiply_reduce_fusion
  19.8 0.9 fusion.88
  20.7 1.1 %fusion.89 = f32[16,512]{1,0:T(8,128)S(1)} fusion(bf16[128,512]{1,0:T(8,128)(2,1)} %param.23, f32[128]{0:T(128)S(1)} %dynamic_slice.11, f32[16]{0:T(128)S(1)} %add_rsqrt_fusion.1, bf16[16,2048]{1,0:T(8,128)(2,1)S(1)} %slice.64, s32[]{:T(128)S(6)} %select_n.48), kind=kOutput, calls=%fused_computation.129 | convolution fusion | flops 2105344 | bytes 168964 | tf_op jit(solution)/shard_map/dot_general | solution.py:85
  21.8 1.2 %fusion.90 = f32[16,1536]{1,0:T(8,128)S(1)} fusion(bf16[128,1536]{1,0:T(8,128)(2,1)} %param.22, f32[128]{0:T(128)S(1)} %dynamic_slice.11, f32[16]{0:T(128)S(1)} %add_rsqrt_fusion.1, bf16[16,2048]{1,0:T(8,128)(2,1)S(1)} %slice.64, s32[]{:T(128)S(6)} %select_n.48), kind=kOutput, calls=%fused_computation.130 | convolution fusion | flops 6299648 | bytes 496644 | tf_op jit(solution)/shard_map/dot_general | solution.py:84
  23.0 0.8 copy.33
  23.8 3.5 %all-to-all-start.1 = ((f32[16,1,2080]{2,1,0:T(1,128)}), f32[16,1,2080]{2,1,0:T(1,128)S(1)}, u32[]{:S(2)}, u32[]{:S(2)}) async-start(f32[16,1,2080]{2,1,0:T(1,128)} %copy.33), calls=%async_computation.1 | async-start | bytes 278528 | tf_op jit(solution)/shard_map/all_to_all | solution.py:90
  27.3 0.2 convolution_select_fusion.1
  27.6 7.7 %all-to-all-done.1 = f32[16,1,2080]{2,1,0:T(1,128)S(1)} async-done(((f32[16,1,2080]{2,1,0:T(1,128)}), f32[16,1,2080]{2,1,0:T(1,128)S(1)}, u32[]{:S(2)}, u32[]{:S(2)}) %all-to-all-start.1) | async-done | bytes 133152 | tf_op jit(solution)/shard_map/all_to_all | solution.py:90
  35.4 0.6 multiply_reduce_fusion.2
  37.1 0.1 tile.13
  37.2 1.6 %convolution_convert_fusion.4 = bf16[16,512]{1,0:T(8,128)(2,1)S(1)} fusion(bf16[512,1024]{1,0:T(8,128)(2,1)} %param.25, bf16[16,1024]{1,0:T(8,128)(2,1)S(1)} %tile.13, s32[1024]{0:T(1024)S(1)} %add_select_fusion), kind=kOutput, calls=%fused_computation.23 | convolution fusion | flops 16818176 | bytes 1101824 | tf_op jit(solution)/shard_map/shm,cm->shc/dot_general | solution.py:128
  38.8 0.1 convolution_bitcast_fusion
  39.0 1.2 %fusion.31 = f32[16,3072]{1,0:T(8,128)S(1)} fusion(bf16[1,32,3072]{2,1,0:T(8,128)(2,1)} %param.20, bf16[16,16]{1,0:T(8,128)(2,1)S(1)} %get-tuple-element.6, bf16[16,16]{1,0:T(8,128)(2,1)S(1)} %get-tuple-element.5), kind=kOutput, calls=%fused_computation.32 | convolution fusion | flops 3147776 | bytes 394240 | tf_op jit(solution)/shard_map/shr,srk->shk/dot_general | solution.py:132
  40.2 1.0 %select_reduce_fusion = (f32[16]{0:T(128)S(1)}, f32[16,3072]{1,0:T(8,128)S(1)}) fusion(pred[3072]{0:T(1024)(128)(4,1)S(1)} %iota_compare_fusion.2, f32[16,3072]{1,0:T(8,128)S(1)} %fusion.31, bf16[16,512]{1,0:T(8,128)(2,1)S(1)} %convolution_convert_fusion.4, bf16[1,3072,512]{2,1,0:T(8,128)(2,1)S(1)} %copy-done), kind=kOutput, calls=%fused_computation.36 | convolution fusion | flops 50528240 | bytes 3558464 | tf_op jit(solution)/shard_map/shc,skc->shk/dot_general | solution.py:131
  41.3 0.2 fusion.96
  41.5 0.2 fusion.33
  41.7 2.0 %fusion.12 = bf16[1024]{0:T(1024)(128)(2,1)S(1)} fusion(bf16[512,1024]{1,0:T(8,128)(2,1)} %param.26, bf16[1,3072,512]{2,1,0:T(8,128)(2,1)S(1)} %copy-done, f32[16,3072]{1,0:T(8,128)S(1)} %get-tuple-element.12, f32[16]{0:T(128)S(1)} %get-tuple-element.8, f32[16]{0:T(128)S(1)} %get-tuple-element.13, pred[3072]{0:T(1024)(128)(4,1)S(1)} %iota_compare_fusion.2, ...), kind=kOutput, calls=%fused_computation.19 | convolution fusion | flops 67378176 | bytes 4402368 | tf_op jit(solution)/shard_map/shc,cm->shm/dot_general | solution.py:149
  43.8 0.7 convert_element_type.183
  44.4 4.0 %all-to-all-start.2 = ((bf16[1,16,64]{2,0,1:T(2,128)(2,1)}), bf16[1,16,64]{2,0,1:T(2,128)(2,1)}, u32[]{:S(2)}, u32[]{:S(2)}) async-start(bf16[1,16,64]{2,0,1:T(2,128)(2,1)} %convert_element_type.183), calls=%async_computation.2 | async-start | bytes 16384 | tf_op jit(solution)/shard_map/all_to_all | solution.py:153
  48.5 0.6 reshape.417
  49.1 5.5 %all-to-all-done.2 = bf16[1,16,64]{2,0,1:T(2,128)(2,1)} async-done(((bf16[1,16,64]{2,0,1:T(2,128)(2,1)}), bf16[1,16,64]{2,0,1:T(2,128)(2,1)}, u32[]{:S(2)}, u32[]{:S(2)}) %all-to-all-start.2) | async-done | bytes 2080 | tf_op jit(solution)/shard_map/all_to_all | solution.py:153
  54.7 1.5 %convolution_convert_fusion = bf16[80,2048]{1,0:T(8,128)(2,1)S(1)} fusion(bf16[64,2048]{1,0:T(8,128)(2,1)} %param.27, pred[80,16]{1,0:T(8,128)(4,1)} %reshape.417, bf16[1,16,64]{2,0,1:T(2,128)(2,1)} %all-to-all-done.2), kind=kOutput, calls=%fused_computation.5 | convolution fusion | flops 21304320 | bytes 593152 | tf_op jit(solution)/shard_map/dot_general | solution.py:156
  56.1 0.9 reshape.422
  57.1 4.4 %all-to-all-start.3 = ((bf16[16,5,2048]{2,1,0:T(8,128)(2,1)}), bf16[16,5,2048]{2,1,0:T(8,128)(2,1)}, u32[]{:S(2)}, u32[]{:S(2)}) async-start(bf16[16,5,2048]{2,1,0:T(8,128)(2,1)} %reshape.422), calls=%async_computation.3 | async-start | bytes 1048576 | tf_op jit(solution)/shard_map/all_to_all | solution.py:157
  61.5 0.6 reduce_sum.90
  62.1 0.6 divide_bitcast_fusion
  62.7 0.7 fusion.67
  63.4 12.3 %all-to-all-done.3 = bf16[16,5,2048]{2,1,0:T(8,128)(2,1)} async-done(((bf16[16,5,2048]{2,1,0:T(8,128)(2,1)}), bf16[16,5,2048]{2,1,0:T(8,128)(2,1)}, u32[]{:S(2)}, u32[]{:S(2)}) %all-to-all-start.3) | async-done | bytes 327712 | tf_op jit(solution)/shard_map/all_to_all | solution.py:157
  75.7 1.2 %convert_reduce_fusion = f32[5,2048]{1,0:T(8,128)S(1)} fusion(bf16[16,5,2048]{2,1,0:T(8,128)(2,1)} %all-to-all-done.3), kind=kLoop, calls=%fused_computation.31 | loop fusion | flops 317440 | bytes 368640 | tf_op jit(solution)/shard_map/reduce_sum | solution.py:160
  76.9 0.1 fusion.97
  77.0 0.1 multiply_reduce_fusion.1
  77.2 2.0 %fusion.10 = f32[4,512]{1,0:T(4,128)S(1)} fusion(bf16[1,2048,512]{2,1,0:T(8,128)(2,1)} %param.33, f32[5,2048]{1,0:T(8,128)S(1)} %get-tuple-element.15, f32[2048]{0:T(1024)} %param.30, f32[4]{0:T(128)S(1)} %slice.74), kind=kOutput, calls=%fused_computation.16 | convolution fusion | flops 8413184 | bytes 2146816 | tf_op jit(solution)/shard_map/dot_general | solution.py:164
  79.3 3.0 %convolution_convert_fusion.2 = bf16[4,2048]{1,0:T(4,128)(2,1)S(1)} fusion(bf16[1,512,2048]{2,1,0:T(8,128)(2,1)} %param.35, bf16[1,2048,512]{2,1,0:T(8,128)(2,1)} %param.34, f32[4,512]{1,0:T(4,128)S(1)} %fusion.10, f32[5,2048]{1,0:T(8,128)S(1)} %get-tuple-element.15, f32[2048]{0:T(1024)S(1)} %copy-done.2, f32[4]{0:T(128)S(1)} %slice.74), kind=kOutput, calls=%fused_computation.10 | convolution fusion | flops 16822272 | bytes 4260352 | tf_op jit(solution)/shard_map/dot_general | solution.py:167
  82.3 0.2 fusion.4
  82.5 0.7 reduce.18
  83.2 0.7 reshape.437
  83.8 4.1 %all-to-all-start.4 = ((bf16[16,2,1024]{2,1,0:T(2,128)(2,1)}), bf16[16,2,1024]{2,1,0:T(2,128)(2,1)S(1)}, u32[]{:S(2)}, u32[]{:S(2)}) async-start(bf16[16,2,1024]{2,1,0:T(2,128)(2,1)} %reshape.437), calls=%async_computation.4 | async-start | bytes 131072 | tf_op jit(solution)/shard_map/all_to_all | solution.py:169
  88.0 0.6 pad_maximum_fusion.3
  88.6 6.2 %all-to-all-done.4 = bf16[16,2,1024]{2,1,0:T(2,128)(2,1)S(1)} async-done(((bf16[16,2,1024]{2,1,0:T(2,128)(2,1)}), bf16[16,2,1024]{2,1,0:T(2,128)(2,1)S(1)}, u32[]{:S(2)}, u32[]{:S(2)}) %all-to-all-start.4) | async-done | bytes 65568 | tf_op jit(solution)/shard_map/all_to_all | solution.py:169
  94.9 0.8 fusion.6
  (59 shorter events, 1.5 us)
Async XLA Ops:
  0.6 39.6 %copy-start = (bf16[1,3072,512]{2,1,0:T(8,128)(2,1)S(1)}, bf16[1,3072,512]{2,1,0:T(8,128)(2,1)}, u32[]{:S(2)}) copy-start(bf16[1,3072,512]{2,1,0:T(8,128)(2,1)} %param.19) | copy-start | bytes 9437188
  0.6 36.4 %copy-start.3 = (f32[512]{0:T(512)S(1)}, f32[512]{0:T(512)}, u32[]{:S(2)}) copy-start(f32[512]{0:T(512)} %param.29) | copy-start | bytes 6148
  4.8 14.4 %all-to-all-start = ((bf16[16,2,1088]{2,1,0:T(2,128)(2,1)}), bf16[16,2,1088]{2,1,0:T(2,128)(2,1)S(1)}, u32[]{:S(2)}, u32[]{:S(2)}) async-start(bf16[16,2,1088]{2,1,0:T(2,128)(2,1)} %reshape.435), calls=%async_computation | async-start | bytes 147456 | tf_op jit(solution)/shard_map/all_to_all | solution.py:73
  23.8 11.5 %all-to-all-start.1 = ((f32[16,1,2080]{2,1,0:T(1,128)}), f32[16,1,2080]{2,1,0:T(1,128)S(1)}, u32[]{:S(2)}, u32[]{:S(2)}) async-start(f32[16,1,2080]{2,1,0:T(1,128)} %copy.33), calls=%async_computation.1 | async-start | bytes 278528 | tf_op jit(solution)/shard_map/all_to_all | solution.py:90
  27.6 20.9 %copy-start.1 = (pred[16,4,16]{2,1,0:T(4,128)(4,1)}, pred[16,4,16]{2,1,0:T(4,128)(4,1)S(1)}, u32[]{:S(2)}) copy-start(pred[16,4,16]{2,1,0:T(4,128)(4,1)S(1)} %broadcast_compare_fusion) | copy-start | bytes 3076
  37.0 4.2 %copy-start.5 = (bf16[1,16]{1,0:T(2,128)(2,1)}, bf16[1,16]{1,0:T(2,128)(2,1)S(1)}, u32[]{:S(2)}) copy-start(bf16[1,16]{1,0:T(2,128)(2,1)S(1)} %get-tuple-element.9) | copy-start | bytes 100
  37.0 4.2 %copy-start.7 = (bf16[1,16]{1,0:T(2,128)(2,1)}, bf16[1,16]{1,0:T(2,128)(2,1)S(1)}, u32[]{:S(2)}) copy-start(bf16[1,16]{1,0:T(2,128)(2,1)S(1)} %get-tuple-element.10) | copy-start | bytes 100
  37.1 4.2 %copy-start.4 = (bf16[1,512]{1,0:T(2,128)(2,1)}, bf16[1,512]{1,0:T(2,128)(2,1)S(1)}, u32[]{:S(2)}) copy-start(bf16[1,512]{1,0:T(2,128)(2,1)S(1)} %get-tuple-element.4) | copy-start | bytes 3076
  43.7 17.7 %copy-start.9 = (f32[1,2]{1,0:T(1,128)S(1)}, f32[1,2]{1,0:T(1,128)}, u32[]{:S(2)}) copy-start(f32[1,2]{1,0:T(1,128)} %param.32) | copy-start | bytes 28
  44.4 10.3 %all-to-all-start.2 = ((bf16[1,16,64]{2,0,1:T(2,128)(2,1)}), bf16[1,16,64]{2,0,1:T(2,128)(2,1)}, u32[]{:S(2)}, u32[]{:S(2)}) async-start(bf16[1,16,64]{2,0,1:T(2,128)(2,1)} %convert_element_type.183), calls=%async_computation.2 | async-start | bytes 16384 | tf_op jit(solution)/shard_map/all_to_all | solution.py:153
  57.1 22.2 %copy-start.2 = (f32[2048]{0:T(1024)S(1)}, f32[2048]{0:T(1024)}, u32[]{:S(2)}) copy-start(f32[2048]{0:T(1024)} %param.30) | copy-start | bytes 24580
  57.1 18.7 %all-to-all-start.3 = ((bf16[16,5,2048]{2,1,0:T(8,128)(2,1)}), bf16[16,5,2048]{2,1,0:T(8,128)(2,1)}, u32[]{:S(2)}, u32[]{:S(2)}) async-start(bf16[16,5,2048]{2,1,0:T(8,128)(2,1)} %reshape.422), calls=%async_computation.3 | async-start | bytes 1048576 | tf_op jit(solution)/shard_map/all_to_all | solution.py:157
  79.3 8.7 %copy-start.10 = (s32[1,2]{1,0:T(1,128)S(1)}, s32[1,2]{1,0:T(1,128)}, u32[]{:S(2)}) copy-start(s32[1,2]{1,0:T(1,128)} %param.31) | copy-start | bytes 28
  79.3 8.8 %copy-start.6 = (bf16[1,16]{1,0:T(2,128)(2,1)S(1)}, bf16[1,16]{1,0:T(2,128)(2,1)}, u32[]{:S(2)}) copy-start(bf16[1,16]{1,0:T(2,128)(2,1)} %copy-done.5) | copy-start | bytes 100
  79.3 8.7 %copy-start.8 = (bf16[1,16]{1,0:T(2,128)(2,1)S(1)}, bf16[1,16]{1,0:T(2,128)(2,1)}, u32[]{:S(2)}) copy-start(bf16[1,16]{1,0:T(2,128)(2,1)} %copy-done.7) | copy-start | bytes 100
  83.8 11.0 %all-to-all-start.4 = ((bf16[16,2,1024]{2,1,0:T(2,128)(2,1)}), bf16[16,2,1024]{2,1,0:T(2,128)(2,1)S(1)}, u32[]{:S(2)}, u32[]{:S(2)}) async-start(bf16[16,2,1024]{2,1,0:T(2,128)(2,1)} %reshape.437), calls=%async_computation.4 | async-start | bytes 131072 | tf_op jit(solution)/shard_map/all_to_all | solution.py:169

commit v2 on v1

--- a/solution.py
+++ b/solution.py
@@ -1,6 +1,8 @@
 import jax
 import jax.numpy as jnp
 from jax import lax
+from jax.experimental import pallas as pl
+from jax.experimental.pallas import tpu as pltpu
 from jax.sharding import PartitionSpec as P
 
 D = 2048
@@ -33,6 +35,55 @@
     return jnp.concatenate(
         [first * cosine - second * sine, second * cosine + first * sine], axis=-1
     )
+
+
+def project_kernel(tokens_ref, cols_ref, gain_ref, wq_ref, wl_ref, wr_ref, tag_ref, out_ref):
+    f32 = jnp.float32
+    wide = tokens_ref[...].astype(f32)
+    scale = lax.rsqrt(jnp.mean(wide * wide, axis=-1, keepdims=True) + EPS)
+    rows = (cols_ref[...].astype(f32) * scale * gain_ref[...]).astype(jnp.bfloat16)
+    q = jnp.dot(rows, wq_ref[...], preferred_element_type=f32)
+    lat = jnp.dot(rows, wl_ref[...], preferred_element_type=f32)
+    last = jnp.dot(rows, wr_ref[...], preferred_element_type=f32) + tag_ref[...]
+    qw, lw = q.shape[1], lat.shape[1]
+    for i in range(rows.shape[0]):
+        out_ref[i, :, 0:qw] = q[i : i + 1]
+        out_ref[i, :, qw : qw + lw] = lat[i : i + 1]
+        out_ref[i, :, qw + lw :] = last[i : i + 1]
+
+
+def expert_kernel(
+    parts_ref, tok_ref, gain_ref, pick_ref, wg_hbm, wu_hbm, wd_hbm,
+    resid_ref, out_ref, x_ref, wg, wu, wd, sems,
+):
+    f32, bf16 = jnp.float32, jnp.bfloat16
+    loads = [
+        pltpu.make_async_copy(src.at[0], dst, sems.at[n])
+        for n, (src, dst) in enumerate(((wg_hbm, wg), (wu_hbm, wu), (wd_hbm, wd)))
+    ]
+    for load in loads:
+        load.start()
+    half = parts_ref.shape[-1]
+    for k in range(parts_ref.shape[1]):
+        part = jnp.sum(parts_ref[:, k].astype(f32), axis=0)
+        x_ref[k : k + 1, 0:half] = part[0:1]
+        x_ref[k : k + 1, half:] = part[1:2]
+    resid = (tok_ref[...] + x_ref[...]).astype(bf16)
+    wide = resid.astype(f32)
+    scale = lax.rsqrt(jnp.mean(wide * wide, axis=-1, keepdims=True) + EPS)
+    rows = (wide * scale * gain_ref[...]).astype(bf16)
+    resid_ref[...] = resid[0 : resid_ref.shape[0]]
+    loads[0].wait()
+    gate = jnp.dot(rows, wg[...], preferred_element_type=f32)
+    loads[1].wait()
+    upper = jnp.dot(rows, wu[...], preferred_element_type=f32)
+    hidden = (gate * jax.nn.sigmoid(gate) * upper).astype(bf16)
+    loads[2].wait()
+    result = jnp.dot(hidden, wd[...], preferred_element_type=f32).astype(bf16)
+    spread = jnp.dot(pick_ref[...], result, preferred_element_type=f32)
+    for i in range(spread.shape[0]):
+        out_ref[i, 0:1, :] = spread[i : i + 1, 0:half].astype(bf16)
+        out_ref[i, 1:2, :] = spread[i : i + 1, half:].astype(bf16)
 
 
 def body(
@@ -66,29 +117,33 @@
     bf16, f32 = jnp.bfloat16, jnp.float32
 
     top_k = routes.shape[1]
-    tagged = jnp.concatenate(
-        [tokens, routes.astype(bf16), jnp.zeros((local_seqs, LANES - top_k), bf16)], axis=1
-    )
-    tagged = jnp.broadcast_to(tagged[None], (devices,) + tagged.shape).reshape(total_rows, -1)
-    gathered = lax.all_to_all(tagged, "ep", split_axis=0, concat_axis=0, tiled=True)
-    all_tokens = gathered[:, :width]
-    all_routes = gathered[:, width : width + top_k].astype(jnp.int32)
-
-    all32 = all_tokens.astype(f32)
-    scale_rows = lax.rsqrt(jnp.mean(all32 * all32, axis=-1, keepdims=True) + EPS)
-    my_cols = lax.dynamic_slice_in_dim(all_tokens, me * block, block, axis=1).astype(f32)
-    my_gain = lax.dynamic_slice_in_dim(gain_attn, me * block, block, axis=0)
-    rows = (my_cols * scale_rows * my_gain).astype(bf16)
-    partial = jnp.concatenate(
-        [
-            jnp.dot(rows, w_query, preferred_element_type=f32),
-            jnp.dot(rows, w_latent, preferred_element_type=f32),
-            jnp.dot(rows, w_rope, preferred_element_type=f32),
-        ],
-        axis=1,
-    )
+    half = width // 2
+    copies = jnp.broadcast_to(
+        tokens.reshape(1, local_seqs, 2, half), (devices, local_seqs, 2, half)
+    ).reshape(total_rows, 2, half)
+    gathered = lax.all_to_all(copies, "ep", split_axis=0, concat_axis=0, tiled=True)
+    all_tokens = gathered.reshape(total_rows, width)
+    my_cols = lax.dynamic_slice_in_dim(all_tokens, me * block, block, axis=1)
+    my_gain = lax.dynamic_slice_in_dim(gain_attn, me * block, block, axis=0)[None]
+    pe_width = w_rope.shape[1]
+    last = pe_width + local_seqs * top_k
+    last += -last % LANES
+    w_last = jnp.pad(w_rope, ((0, 0), (0, last - pe_width)))
+    tag = jnp.pad(
+        routes.reshape(1, -1).astype(f32),
+        ((0, 0), (pe_width, last - pe_width - local_seqs * top_k)),
+    )
+    sum_width = q_width + lat_width + pe_width
+    partial = pl.pallas_call(
+        project_kernel,
+        out_shape=jax.ShapeDtypeStruct((total_rows, 1, q_width + lat_width + last), f32),
+        name="project",
+    )(all_tokens, my_cols, my_gain, w_query, w_latent, w_last, tag)
     partial = lax.all_to_all(partial, "ep", split_axis=0, concat_axis=0, tiled=True)
-    summed = jnp.sum(partial.reshape(devices, local_seqs, -1), axis=0)
+    partial = partial.reshape(devices, local_seqs, -1)
+    summed = jnp.sum(partial[:, :, :sum_width], axis=0)
+    all_routes = partial[:, 0, sum_width : sum_width + local_seqs * top_k]
+    all_routes = all_routes.reshape(total_rows, top_k).astype(jnp.int32)
 
     token_ids = jnp.arange(total_rows)
     expert_ids = jnp.arange(devices)
@@ -106,7 +161,7 @@
     per = local_seqs + CAP
     sel_mine = lax.dynamic_slice_in_dim(sel, me, 1, axis=0)[0]
     tokens_mine = jnp.dot(sel_mine, all_tokens, preferred_element_type=f32)
-    picker = sel_mine[local_seqs:]
+    pick = jnp.where(jnp.arange(per)[None, :] >= local_seqs, sel_mine.T, jnp.zeros((), bf16))
     hits = routes[:, :, None] == expert_ids[None, None, :]
     route_weight = route_scores / jnp.sum(route_scores, axis=-1, keepdims=True)
     weight_table = jnp.sum(hits.astype(f32) * route_weight[:, :, None], axis=1)
@@ -155,21 +210,32 @@
                      preferred_element_type=f32).astype(bf16)
     out_part = jnp.dot(picked, w_output, preferred_element_type=f32).astype(bf16)
     out_part = lax.all_to_all(
-        out_part.reshape(devices, per, width), "ep", split_axis=0, concat_axis=0, tiled=True
-    )
-    attn_out = jnp.sum(out_part.astype(f32), axis=0)
-    resid = (tokens_mine + attn_out).astype(bf16)
-    moe_in = rms_scale(resid.astype(f32), gain_moe).astype(bf16)
-    packed = moe_in[local_seqs:]
-    gate = jnp.dot(packed, w_gate[0], preferred_element_type=f32)
-    upper = jnp.dot(packed, w_up[0], preferred_element_type=f32)
-    hidden = (jax.nn.silu(gate) * upper).astype(bf16)
-    result = jnp.dot(hidden, w_down[0], preferred_element_type=f32).astype(bf16)
-    spread = jnp.dot(picker.T, result, preferred_element_type=f32).astype(bf16)
+        out_part.reshape(devices, per, 2, half), "ep", split_axis=0, concat_axis=0, tiled=True
+    )
+    ff = w_gate.shape[2]
+    whole = pl.BlockSpec(memory_space=pltpu.VMEM)
+    far = pl.BlockSpec(memory_space=pl.ANY)
+    resid, spread = pl.pallas_call(
+        expert_kernel,
+        out_shape=(
+            jax.ShapeDtypeStruct((local_seqs, width), bf16),
+            jax.ShapeDtypeStruct((total_rows, 2, half), bf16),
+        ),
+        in_specs=[whole] * 4 + [far] * 3,
+        out_specs=(whole, whole),
+        scratch_shapes=[
+            pltpu.VMEM((per, width), f32),
+            pltpu.VMEM((width, ff), bf16),
+            pltpu.VMEM((width, ff), bf16),
+            pltpu.VMEM((ff, width), bf16),
+            pltpu.SemaphoreType.DMA((3,)),
+        ],
+        name="experts",
+    )(out_part, tokens_mine, gain_moe[None], pick, w_gate, w_up, w_down)
     answers = lax.all_to_all(spread, "ep", split_axis=0, concat_axis=0, tiled=True)
     answers = answers.reshape(devices, local_seqs, width)
     moe_sum = jnp.einsum("sn,nsd->sd", weight_table, answers.astype(f32))
-    mixed = (resid[:local_seqs].astype(f32) + moe_sum).astype(bf16)
+    mixed = (resid.astype(f32) + moe_sum).astype(bf16)
     return (mixed, new_latent, new_rope)
 
 

time: 96.6 us -> 87.4 us (0.905)
  waiting for transfers between devices: 37.3 us -> 24.2 us
  matrix products: 17.1 us -> 9.02 us
  Pallas kernels: 0 us -> 7.1 us
  other arithmetic: 8.09 us -> 11.8 us
  local copies, waits for them, and re-layouts: 7.48 us -> 9.37 us
    all_to_all x2, waiting for transfers between devices: 17.8 us -> 8.19 us  [the longest x1 6.56 us: body(): lax.all_to_all(out_part.reshape(devices, per, 2, half), 'ep', split_axis=...]
    dot_general x6 -> x0, matrix products: 8.42 us -> none  [the longest x1 2.99 us: body(): result = jnp.dot(hidden, w_down[0], preferred_element_type=f32).astype(bf16)]
    pallas_call x0 -> x2, Pallas kernels: none -> 7.1 us  [the longest x1 5.06 us: body(): pl.pallas_call(expert_kernel, out_shape=(jax.ShapeDtypeStruct((local_seqs...]
    all_to_all x1, waiting for transfers between devices: 7.73 us -> 4.36 us  [body(): lax.all_to_all(partial, 'ep', split_axis=0, concat_axis=0, tiled=True)]
    squeeze x0 -> x1, local copies, waits for them, and re-layouts: none -> 1.34 us  [body(): sel_mine = lax.dynamic_slice_in_dim(sel, me, 1, axis=0)[0]]
    reduce_sum x3 -> x1, other arithmetic: 1.39 us -> 0.08 us  [body(): summed = jnp.sum(partial[:, :, :sum_width], axis=0)]
    broadcast_in_dim x1 -> x2, local copies, waits for them, and re-layouts: 0.01 us -> 1.28 us  [the longest x1 1.27 us: body(): lax.dynamic_slice_in_dim(gain_attn, me * block, block, axis=0)[None]]
    select_n x0 -> x1, other arithmetic: none -> 1.28 us  [body(): jnp.where(jnp.arange(per)[None, :] >= local_seqs, sel_mine.T, jnp.zeros((...]
  transfers between devices with their start and end apart: 5 -> 5, of which waited for: 5 -> 5; matrix products, arithmetic and copies ran while one was open for 5% -> 16% of each run, Pallas kernels for 0% -> 0%
where the time goes in v2:
time: 87.4 us; the launch traced here: 86.5 us
  waiting for transfers between devices  24.2 us (28%)
  starting transfers between devices  22.9 us (26%)
  other arithmetic  11.8 us (14%)
  local copies, waits for them, and re-layouts  9.37 us (11%)
  matrix products  9.02 us (10%)
  Pallas kernels  7.1 us (8%)
  between operations  2.25 us (3%)
    all_to_all x1, starting transfers between devices, body(): lax.all_to_all(copies, 'ep', split_axis=0, concat_axis=0, tiled=True)  7.41 us
    all_to_all x1, waiting for transfers between devices, body(): lax.all_to_all(out_part.reshape(devices, per, 2, half), 'ep', split_axis=...  6.56 us
    all_to_all x1, waiting for transfers between devices, body(): lax.all_to_all(spread, 'ep', split_axis=0, concat_axis=0, tiled=True)  6.16 us
    all_to_all x1, waiting for transfers between devices, body(): lax.all_to_all(values, 'ep', split_axis=1, concat_axis=0, tiled=True)  5.46 us
    pallas_call x1, Pallas kernels, body(): pl.pallas_call(expert_kernel, out_shape=(jax.ShapeDtypeStruct((local_seqs...  5.06 us
    all_to_all x1, starting transfers between devices, body(): lax.all_to_all(partial, 'ep', split_axis=0, concat_axis=0, tiled=True)  4.38 us
    all_to_all x1, waiting for transfers between devices, body(): lax.all_to_all(partial, 'ep', split_axis=0, concat_axis=0, tiled=True)  4.36 us
    all_to_all x1, starting transfers between devices, body(): lax.all_to_all(values, 'ep', split_axis=1, concat_axis=0, tiled=True)  4.04 us
  transfers between devices with their start and end apart: 5, of which 5 were waited for; matrix products, arithmetic and copies ran while one was open for 16% of the time, Pallas kernels for 0%

profile of v2, /device:TPU:0, one launch (start us, length us, event | category | flops | bytes accessed | tf_op | source)
XLA Modules:
  0.0 86.5 jit_solution(14201672702305318691)
XLA Ops:
  0.7 0.9 %reduce.10 = bf16[2048]{0:T(1024)(128)(2,1)S(1)} reduce(bf16[1,2048]{1,0:T(2,128)(2,1)} %param.18, bf16[]{:T(256)} %constant.75), dimensions={0}, to_apply=%param.18.reduce_sub_computation | reduce | bytes 8194 | tf_op args[0]
  1.6 0.7 reshape.399
  2.2 7.4 %all-to-all-start = ((bf16[16,2,1024]{2,1,0:T(2,128)(2,1)}), bf16[16,2,1024]{2,1,0:T(2,128)(2,1)S(1)}, u32[]{:S(2)}, u32[]{:S(2)}) async-start(bf16[16,2,1024]{2,1,0:T(2,128)(2,1)} %reshape.399), calls=%async_computation | async-start | bytes 131072 | tf_op jit(solution)/shard_map/all_to_all | solution.py:124
  10.3 0.6 fusion.55
  11.0 1.3 %dynamic-slice_bitcast_fusion.gain_ref = f32[1,128]{1,0:T(1,128)} fusion(f32[2048]{0:T(1024)} %param.28, s32[]{:T(128)S(6)} %select_n.51), kind=kLoop, calls=%fused_computation.92 | loop fusion | bytes 1028 | tf_op jit(solution)/shard_map/broadcast_in_dim | solution.py:127
  12.2 0.7 convert_element_type.135
  12.9 0.8 copy.43
  13.7 0.6 pad.9.tag_ref
  14.3 0.6 pad.8.wr_ref
  14.9 1.6 %all-to-all-done = bf16[16,2,1024]{2,1,0:T(2,128)(2,1)S(1)} async-done(((bf16[16,2,1024]{2,1,0:T(2,128)(2,1)}), bf16[16,2,1024]{2,1,0:T(2,128)(2,1)S(1)}, u32[]{:S(2)}, u32[]{:S(2)}) %all-to-all-start) | async-done | bytes 65568 | tf_op jit(solution)/shard_map/all_to_all | solution.py:124
  16.6 0.6 constant_dynamic-slice_fusion.cols_ref
  17.2 2.0 %project.1 = f32[16,1,2176]{2,1,0:T(1,128)} custom-call(bf16[16,2048]{1,0:T(8,128)(2,1)} %bitcast.81, bf16[16,128]{1,0:T(8,128)(2,1)} %constant_dynamic-slice_fusion.cols_ref, f32[1,128]{1,0:T(1,128)} %dynamic-slice_bitcast_fusion.gain_ref, bf16[128,1536]{1,0:T(8,128)(2,1)} %wq_ref.1, bf16[128,512]{1,0:T(8,128)(2,1)} %wl_ref.1, bf16[128,128]{1,0:T(8,128)(2,1)} %pad.8.wr_ref, ...), custom_call_target="tpu_custom_call" | custom-call | tf_op jit(solution)/shard_map/project/pallas_call | solution.py:137
  19.2 4.4 %all-to-all-start.1 = ((f32[16,1,2176]{2,1,0:T(1,128)}), f32[16,1,2176]{2,1,0:T(1,128)S(1)}, u32[]{:S(2)}, u32[]{:S(2)}) async-start(f32[16,1,2176]{2,1,0:T(1,128)} %project.1), calls=%async_computation.1 | async-start | bytes 278528 | tf_op jit(solution)/shard_map/all_to_all | solution.py:142
  23.6 0.5 iota_convert_fusion
  24.1 1.3 %reduce_sum.61 = f32[]{:T(128)} reduce(f32[1,2]{1,0:T(1,128)} %param.32, f32[]{:T(128)} %constant.47.clone.1), dimensions={0,1}, to_apply=%region_6.7 | reduce | flops 1 | bytes 16 | tf_op jit(solution)/shard_map/reduce_sum | solution.py:166
  25.4 1.9 %divide_bitcast_fusion = f32[2]{0:T(128)} fusion(f32[1,2]{1,0:T(1,128)} %param.32, f32[]{:T(128)} %reduce_sum.61), kind=kLoop, calls=%fused_computation.83 | loop fusion | flops 2 | bytes 20 | tf_op jit(solution)/shard_map/div | solution.py:166
  27.3 4.4 %all-to-all-done.1 = f32[16,1,2176]{2,1,0:T(1,128)S(1)} async-done(((f32[16,1,2176]{2,1,0:T(1,128)}), f32[16,1,2176]{2,1,0:T(1,128)S(1)}, u32[]{:S(2)}, u32[]{:S(2)}) %all-to-all-start.1) | async-done | bytes 139296 | tf_op jit(solution)/shard_map/all_to_all | solution.py:142
  31.8 0.6 multiply_reduce_fusion
  33.7 0.7 fusion.64
  34.4 0.2 convolution_select_fusion.1
  34.6 0.1 tile.13
  34.7 1.6 %convolution_convert_fusion.2 = bf16[16,512]{1,0:T(8,128)(2,1)S(1)} fusion(bf16[512,1024]{1,0:T(8,128)(2,1)} %param.25, bf16[16,1024]{1,0:T(8,128)(2,1)S(1)} %tile.13, s32[1024]{0:T(1024)S(1)} %add_select_fusion), kind=kOutput, calls=%fused_computation.13 | convolution fusion | flops 16818176 | bytes 1101824 | tf_op jit(solution)/shard_map/shm,cm->shc/dot_general | solution.py:183
  36.3 0.1 convolution_bitcast_fusion
  36.4 0.8 fusion.37
  37.2 0.2 fusion.16
  37.4 1.0 %select_reduce_fusion = (f32[16]{0:T(128)S(1)}, f32[16,3072]{1,0:T(8,128)S(1)}) fusion(pred[3072]{0:T(1024)(128)(4,1)S(1)} %iota_compare_fusion.2, f32[16,3072]{1,0:T(8,128)S(1)} %fusion.16, bf16[16,512]{1,0:T(8,128)(2,1)S(1)} %convolution_convert_fusion.2, bf16[1,3072,512]{2,1,0:T(8,128)(2,1)S(1)} %copy-done), kind=kOutput, calls=%fused_computation.23 | convolution fusion | flops 50528240 | bytes 3558464 | tf_op jit(solution)/shard_map/shc,skc->shk/dot_general | solution.py:186
  38.5 0.2 fusion.65
  38.7 0.2 fusion.18
  38.9 2.1 %fusion.5 = bf16[1024]{0:T(1024)(128)(2,1)S(1)} fusion(bf16[512,1024]{1,0:T(8,128)(2,1)} %param.26, bf16[1,3072,512]{2,1,0:T(8,128)(2,1)S(1)} %copy-done, f32[16,3072]{1,0:T(8,128)S(1)} %get-tuple-element.16, f32[16]{0:T(128)S(1)} %get-tuple-element.12, f32[16]{0:T(128)S(1)} %get-tuple-element.17, pred[3072]{0:T(1024)(128)(4,1)S(1)} %iota_compare_fusion.2, ...), kind=kOutput, calls=%fused_computation.9 | convolution fusion | flops 67378176 | bytes 4402368 | tf_op jit(solution)/shard_map/shc,cm->shm/dot_general | solution.py:204
  41.0 0.7 convert_element_type.158
  41.7 4.0 %all-to-all-start.2 = ((bf16[1,16,64]{2,0,1:T(2,128)(2,1)}), bf16[1,16,64]{2,0,1:T(2,128)(2,1)}, u32[]{:S(2)}, u32[]{:S(2)}) async-start(bf16[1,16,64]{2,0,1:T(2,128)(2,1)} %convert_element_type.158), calls=%async_computation.2 | async-start | bytes 16384 | tf_op jit(solution)/shard_map/all_to_all | solution.py:208
  45.9 0.6 reshape.401
  46.5 5.5 %all-to-all-done.2 = bf16[1,16,64]{2,0,1:T(2,128)(2,1)} async-done(((bf16[1,16,64]{2,0,1:T(2,128)(2,1)}), bf16[1,16,64]{2,0,1:T(2,128)(2,1)}, u32[]{:S(2)}, u32[]{:S(2)}) %all-to-all-start.2) | async-done | bytes 2080 | tf_op jit(solution)/shard_map/all_to_all | solution.py:208
  52.0 1.5 %convolution_convert_fusion = bf16[80,2048]{1,0:T(8,128)(2,1)S(1)} fusion(bf16[64,2048]{1,0:T(8,128)(2,1)} %param.27, pred[80,16]{1,0:T(8,128)(4,1)} %reshape.401, bf16[1,16,64]{2,0,1:T(2,128)(2,1)} %all-to-all-done.2), kind=kOutput, calls=%fused_computation.5 | convolution fusion | flops 21304320 | bytes 593152 | tf_op jit(solution)/shard_map/dot_general | solution.py:211
  53.4 0.9 %reshape.406 = bf16[16,5,2,1024]{3,2,1,0:T(2,128)(2,1)} reshape(bf16[80,2048]{1,0:T(8,128)(2,1)S(1)} %convolution_convert_fusion) | data formatting | bytes 655360 | tf_op jit(solution)/shard_map/reshape | solution.py:213
  54.4 3.5 %all-to-all-start.3 = ((bf16[16,5,2,1024]{3,2,1,0:T(2,128)(2,1)}), bf16[16,5,2,1024]{3,2,1,0:T(2,128)(2,1)S(1)}, u32[]{:S(2)}, u32[]{:S(2)}) async-start(bf16[16,5,2,1024]{3,2,1,0:T(2,128)(2,1)} %reshape.406), calls=%async_computation.3 | async-start | bytes 655360 | tf_op jit(solution)/shard_map/all_to_all | solution.py:212
  57.9 0.5 iota_compare_fusion.6
  58.4 0.6 convert_bitcast_fusion
  59.0 1.3 %copy.47 = bf16[5,16]{0,1:T(8,128)(2,1)} copy(bf16[5,16]{1,0:T(8,128)(2,1)} %convert_bitcast_fusion) | data formatting | bytes 320 | tf_op jit(solution)/shard_map/squeeze | solution.py:162
  60.4 1.3 %select_bitcast_fusion.pick_ref = bf16[16,5]{1,0:T(8,128)(2,1)} fusion(bf16[5,16]{0,1:T(8,128)(2,1)} %copy.47, pred[5]{0:T(512)(128)(4,1)} %iota_compare_fusion.6), kind=kLoop, calls=%fused_computation.64 | loop fusion | flops 80 | bytes 325 | tf_op jit(solution)/shard_map/jit(_where)/select_n | solution.py:164
  61.6 0.7 fusion.46.tok_ref
  62.4 6.6 %all-to-all-done.3.parts_ref = bf16[16,5,2,1024]{3,2,1,0:T(2,128)(2,1)S(1)} async-done(((bf16[16,5,2,1024]{3,2,1,0:T(2,128)(2,1)}), bf16[16,5,2,1024]{3,2,1,0:T(2,128)(2,1)S(1)}, u32[]{:S(2)}, u32[]{:S(2)}) %all-to-all-start.3) | async-done | bytes 327712 | tf_op jit(solution)/shard_map/all_to_all | solution.py:212
  68.9 0.7 copy-done.1
  69.7 5.1 %experts.1 = (bf16[1,2048]{1,0:T(2,128)(2,1)}, bf16[16,2,1024]{2,1,0:T(2,128)(2,1)}) custom-call(bf16[16,5,2,1024]{3,2,1,0:T(2,128)(2,1)} %copy-done.1, f32[5,2048]{1,0:T(8,128)} %fusion.46.tok_ref, f32[1,2048]{1,0:T(1,128)} %bitcast.86, bf16[16,5]{1,0:T(8,128)(2,1)} %select_bitcast_fusion.pick_ref, bf16[1,2048,512]{2,1,0:T(8,128)(2,1)} %wg_hbm.1, ...), custom_call_target="tpu_custom_call" | custom-call | tf_op jit(solution)/shard_map/experts/pallas_call | solution.py:218
  74.7 3.5 %all-to-all-start.4 = ((bf16[16,2,1024]{2,1,0:T(2,128)(2,1)}), bf16[16,2,1024]{2,1,0:T(2,128)(2,1)S(1)}, u32[]{:S(2)}, u32[]{:S(2)}) async-start(bf16[16,2,1024]{2,1,0:T(2,128)(2,1)} %get-tuple-element.6), calls=%async_computation.4 | async-start | bytes 131072 | tf_op jit(solution)/shard_map/all_to_all | solution.py:235
  78.4 0.6 pad_maximum_fusion.3
  78.9 6.2 %all-to-all-done.4 = bf16[16,2,1024]{2,1,0:T(2,128)(2,1)S(1)} async-done(((bf16[16,2,1024]{2,1,0:T(2,128)(2,1)}), bf16[16,2,1024]{2,1,0:T(2,128)(2,1)S(1)}, u32[]{:S(2)}, u32[]{:S(2)}) %all-to-all-start.4) | async-done | bytes 65568 | tf_op jit(solution)/shard_map/all_to_all | solution.py:235
  85.1 1.4 %fusion.4 = bf16[1,2048]{1,0:T(2,128)(2,1)} fusion(bf16[16,2048]{1,0:T(8,128)(2,1)S(1)} %bitcast.85, bf16[1,2048]{1,0:T(2,128)(2,1)} %get-tuple-element.5, bf16[16]{0:T(256)(128)(2,1)S(1)} %fusion.49), kind=kOutput, calls=%fused_computation.7 | convolution fusion | flops 71680 | bytes 73760 | tf_op jit(solution)/shard_map/sn,nsd->sd/dot_general | solution.py:237
  (49 shorter events, 1.1 us)
Async XLA Ops:
  0.6 36.8 %copy-start = (bf16[1,3072,512]{2,1,0:T(8,128)(2,1)S(1)}, bf16[1,3072,512]{2,1,0:T(8,128)(2,1)}, u32[]{:S(2)}) copy-start(bf16[1,3072,512]{2,1,0:T(8,128)(2,1)} %param.19) | copy-start | bytes 9437188
  0.6 36.6 %copy-start.4 = (bf16[1,32,3072]{2,1,0:T(8,128)(2,1)S(1)}, bf16[1,32,3072]{2,1,0:T(8,128)(2,1)}, u32[]{:S(2)}) copy-start(bf16[1,32,3072]{2,1,0:T(8,128)(2,1)} %param.20) | copy-start | bytes 589828
  2.2 14.3 %all-to-all-start = ((bf16[16,2,1024]{2,1,0:T(2,128)(2,1)}), bf16[16,2,1024]{2,1,0:T(2,128)(2,1)S(1)}, u32[]{:S(2)}, u32[]{:S(2)}) async-start(bf16[16,2,1024]{2,1,0:T(2,128)(2,1)} %reshape.399), calls=%async_computation | async-start | bytes 131072 | tf_op jit(solution)/shard_map/all_to_all | solution.py:124
  16.6 0.6 copy-start.2
  19.2 12.4 %all-to-all-start.1 = ((f32[16,1,2176]{2,1,0:T(1,128)}), f32[16,1,2176]{2,1,0:T(1,128)S(1)}, u32[]{:S(2)}, u32[]{:S(2)}) async-start(f32[16,1,2176]{2,1,0:T(1,128)} %project.1), calls=%async_computation.1 | async-start | bytes 278528 | tf_op jit(solution)/shard_map/all_to_all | solution.py:142
  33.7 7.3 %copy-start.6 = (bf16[1,16]{1,0:T(2,128)(2,1)}, bf16[1,16]{1,0:T(2,128)(2,1)S(1)}, u32[]{:S(2)}) copy-start(bf16[1,16]{1,0:T(2,128)(2,1)S(1)} %get-tuple-element.13) | copy-start | bytes 100
  33.7 7.3 %copy-start.8 = (bf16[1,16]{1,0:T(2,128)(2,1)}, bf16[1,16]{1,0:T(2,128)(2,1)S(1)}, u32[]{:S(2)}) copy-start(bf16[1,16]{1,0:T(2,128)(2,1)S(1)} %get-tuple-element.14) | copy-start | bytes 100
  34.4 2.8 %copy-start.5 = (bf16[1,512]{1,0:T(2,128)(2,1)}, bf16[1,512]{1,0:T(2,128)(2,1)S(1)}, u32[]{:S(2)}) copy-start(bf16[1,512]{1,0:T(2,128)(2,1)S(1)} %get-tuple-element.8) | copy-start | bytes 3076
  38.5 7.3 %copy-start.10 = (f32[4]{0:T(128)S(1)}, f32[4]{0:T(128)}, u32[]{:S(2)}) copy-start(f32[4]{0:T(128)} %iota_convert_fusion) | copy-start | bytes 52
  38.9 22.7 %copy-start.3 = (bf16[2,8,2,1024]{3,1,2,0:T(8,128)(2,1)S(1)}, bf16[2,8,2,1024]{3,1,2,0:T(8,128)(2,1)}, u32[]{:S(2)}) copy-start(bf16[2,8,2,1024]{3,1,2,0:T(8,128)(2,1)} %copy-done.2) | copy-start | bytes 196612
  41.7 10.3 %all-to-all-start.2 = ((bf16[1,16,64]{2,0,1:T(2,128)(2,1)}), bf16[1,16,64]{2,0,1:T(2,128)(2,1)}, u32[]{:S(2)}, u32[]{:S(2)}) async-start(bf16[1,16,64]{2,0,1:T(2,128)(2,1)} %convert_element_type.158), calls=%async_computation.2 | async-start | bytes 16384 | tf_op jit(solution)/shard_map/all_to_all | solution.py:208
  54.4 14.6 %all-to-all-start.3 = ((bf16[16,5,2,1024]{3,2,1,0:T(2,128)(2,1)}), bf16[16,5,2,1024]{3,2,1,0:T(2,128)(2,1)S(1)}, u32[]{:S(2)}, u32[]{:S(2)}) async-start(bf16[16,5,2,1024]{3,2,1,0:T(2,128)(2,1)} %reshape.406), calls=%async_computation.3 | async-start | bytes 655360 | tf_op jit(solution)/shard_map/all_to_all | solution.py:212
  68.9 0.7 copy-start.1
  69.7 8.6 %copy-start.11 = (s32[1,2]{1,0:T(1,128)S(1)}, s32[1,2]{1,0:T(1,128)}, u32[]{:S(2)}) copy-start(s32[1,2]{1,0:T(1,128)} %param.31) | copy-start | bytes 28
  69.7 8.6 %copy-start.12 = (f32[2]{0:T(128)S(1)}, f32[2]{0:T(128)}, u32[]{:S(2)}) copy-start(f32[2]{0:T(128)} %divide_bitcast_fusion) | copy-start | bytes 28
  69.7 8.7 %copy-start.7 = (bf16[1,16]{1,0:T(2,128)(2,1)S(1)}, bf16[1,16]{1,0:T(2,128)(2,1)}, u32[]{:S(2)}) copy-start(bf16[1,16]{1,0:T(2,128)(2,1)} %copy-done.6) | copy-start | bytes 100
  69.7 8.7 %copy-start.9 = (bf16[1,16]{1,0:T(2,128)(2,1)S(1)}, bf16[1,16]{1,0:T(2,128)(2,1)}, u32[]{:S(2)}) copy-start(bf16[1,16]{1,0:T(2,128)(2,1)} %copy-done.8) | copy-start | bytes 100
  74.7 10.4 %all-to-all-start.4 = ((bf16[16,2,1024]{2,1,0:T(2,128)(2,1)}), bf16[16,2,1024]{2,1,0:T(2,128)(2,1)S(1)}, u32[]{:S(2)}, u32[]{:S(2)}) async-start(bf16[16,2,1024]{2,1,0:T(2,128)(2,1)} %get-tuple-element.6), calls=%async_computation.4 | async-start | bytes 131072 | tf_op jit(solution)/shard_map/all_to_all | solution.py:235

commit v3 on v2

--- a/solution.py
+++ b/solution.py
@@ -86,6 +86,91 @@
         out_ref[i, 1:2, :] = spread[i : i + 1, half:].astype(bf16)
 
 
+def attend_kernel(
+    part_ref, gain_ref, cos_ref, sin_ref, len_ref, wa_hbm, wv_hbm, rope_hbm, lat_hbm,
+    val_ref, newlat_ref, newrope_ref, q_ref, wa, wv, rope, lat, sems,
+):
+    f32, bf16 = jnp.float32, jnp.bfloat16
+    seqs = newlat_ref.shape[0]
+    devices = part_ref.shape[0] // seqs
+    qw = HEADS * (NOPE + ROPE)
+    lw = newlat_ref.shape[1]
+    scale = (NOPE + ROPE) ** (-0.5)
+    half = ROPE // 2
+    load_wa = pltpu.make_async_copy(wa_hbm, wa, sems.at[0])
+    load_wv = pltpu.make_async_copy(wv_hbm, wv, sems.at[1])
+    load_wa.start()
+
+    def turn(v, cosine, sine):
+        first, second = v[:, :half], v[:, half:]
+        return jnp.concatenate(
+            [first * cosine - second * sine, second * cosine + first * sine], axis=1
+        ).astype(bf16)
+
+    def own_lanes(size, each):
+        row = lax.broadcasted_iota(jnp.int32, (HEADS, size), 0)
+        lane = lax.broadcasted_iota(jnp.int32, (HEADS, size), 1)
+        return (lane >= row * each) & (lane < row * each + each)
+
+    for s in range(seqs):
+        load_rope = pltpu.make_async_copy(rope_hbm.at[s], rope, sems.at[2])
+        load_lat = pltpu.make_async_copy(lat_hbm.at[s], lat, sems.at[3])
+        load_rope.start()
+        load_lat.start()
+        if s == 0:
+            load_wv.start()
+        total = part_ref[s]
+        for d in range(1, devices):
+            total = total + part_ref[d * seqs + s]
+        total = total.astype(bf16).astype(f32)
+        cosine, sine = cos_ref[s : s + 1], sin_ref[s : s + 1]
+        raw = total[:, qw : qw + lw]
+        norm = lax.rsqrt(jnp.mean(raw * raw, axis=-1, keepdims=True) + EPS)
+        new_latent = (raw * norm * gain_ref[...]).astype(bf16)
+        new_rope = turn(total[:, qw + lw : qw + lw + ROPE], cosine, sine)
+        newlat_ref[s : s + 1] = new_latent
+        newrope_ref[s : s + 1] = new_rope
+        each = NOPE + ROPE
+        for h in range(HEADS):
+            q_ref[h : h + 1, 0:each] = total[:, h * each : h * each + each]
+        q = q_ref[:, 0:each]
+        q_pe = turn(q[:, NOPE:], cosine, sine)
+        spread = jnp.concatenate([q[:, :NOPE]] * HEADS, axis=1)
+        spread = jnp.where(own_lanes(HEADS * NOPE, NOPE), spread, 0.0).astype(bf16)
+        if s == 0:
+            load_wa.wait()
+        nt = (((1,), (1,)), ((), ()))
+        q_abs = lax.dot_general(spread, wa[...], nt, preferred_element_type=f32).astype(bf16)
+        fresh = (
+            jnp.sum(q_abs.astype(f32) * new_latent.astype(f32), axis=1, keepdims=True)
+            + jnp.sum(q_pe.astype(f32) * new_rope.astype(f32), axis=1, keepdims=True)
+        ) * scale
+        load_rope.wait()
+        past = jnp.dot(q_pe, rope[...], preferred_element_type=f32)
+        load_lat.wait()
+        past = (past + lax.dot_general(q_abs, lat[...], nt, preferred_element_type=f32)) * scale
+        valid = lax.broadcasted_iota(jnp.int32, past.shape, 1) < len_ref[s]
+        top = jnp.max(jnp.where(valid, past, -jnp.inf), axis=1, keepdims=True)
+        top = jnp.maximum(top, fresh)
+        e_past = jnp.where(valid, jnp.exp(past - top), 0.0)
+        e_new = jnp.exp(fresh - top)
+        denom = jnp.sum(e_past, axis=1, keepdims=True) + e_new
+        p_past = (e_past / denom).astype(bf16)
+        p_new = (e_new / denom).astype(bf16).astype(f32)
+        attended = (
+            jnp.dot(p_past, lat[...], preferred_element_type=f32)
+            + p_new * new_latent.astype(f32)
+        ).astype(bf16)
+        if s == 0:
+            load_wv.wait()
+        mixed = jnp.dot(attended, wv[...], preferred_element_type=f32)
+        mixed = jnp.where(own_lanes(HEADS * VDIM, VDIM), mixed, 0.0)
+        values = jnp.sum(mixed, axis=0, keepdims=True).astype(bf16)
+        part = val_ref.shape[2]
+        for d in range(devices):
+            val_ref[d, s : s + 1, :] = values[:, d * part : d * part + part]
+
+
 def body(
     tokens,
     cache_latent,
@@ -140,8 +225,8 @@
         name="project",
     )(all_tokens, my_cols, my_gain, w_query, w_latent, w_last, tag)
     partial = lax.all_to_all(partial, "ep", split_axis=0, concat_axis=0, tiled=True)
+    arrived = partial
     partial = partial.reshape(devices, local_seqs, -1)
-    summed = jnp.sum(partial[:, :, :sum_width], axis=0)
     all_routes = partial[:, 0, sum_width : sum_width + local_seqs * top_k]
     all_routes = all_routes.reshape(total_rows, top_k).astype(jnp.int32)
 
@@ -166,46 +251,32 @@
     route_weight = route_scores / jnp.sum(route_scores, axis=-1, keepdims=True)
     weight_table = jnp.sum(hits.astype(f32) * route_weight[:, :, None], axis=1)
 
-    query = summed[:, :q_width].astype(bf16)
-    latent_raw = summed[:, q_width : q_width + lat_width].astype(bf16)
-    rope_raw = summed[:, q_width + lat_width :].astype(bf16)
-    new_latent = rms_scale(latent_raw.astype(f32), gain_latent).astype(bf16)
     cosine, sine = rope_tables(lengths, ROPE)
-    new_rope = apply_rope(rope_raw.astype(f32), cosine, sine).astype(bf16)
-    heads_view = query.reshape(local_seqs, heads, NOPE + ROPE)
-    q_nope = heads_view[:, :, :NOPE]
-    q_pe = apply_rope(
-        heads_view[:, :, NOPE:].astype(f32), cosine[:, None, :], sine[:, None, :]
-    ).astype(bf16)
-    head_ids = jnp.arange(heads)
-    own_key = (jnp.arange(heads * NOPE) // NOPE)[None, None, :] == head_ids[None, :, None]
-    spread_q = jnp.where(own_key, jnp.tile(q_nope, (1, 1, heads)), jnp.zeros((), bf16))
-    q_abs = jnp.einsum("shm,cm->shc", spread_q, w_absorb, preferred_element_type=f32).astype(bf16)
-    scale = (NOPE + ROPE) ** (-0.5)
-    past = (
-        jnp.einsum("shc,skc->shk", q_abs, cache_latent, preferred_element_type=f32)
-        + jnp.einsum("shr,srk->shk", q_pe, cache_rope, preferred_element_type=f32)
-    ) * scale
-    fresh = (
-        jnp.einsum("shc,sc->sh", q_abs, new_latent, preferred_element_type=f32)
-        + jnp.einsum("shr,sr->sh", q_pe, new_rope, preferred_element_type=f32)
-    ) * scale
-    valid = jnp.arange(cache_latent.shape[1])[None, None, :] < lengths[:, None, None]
-    top = jnp.maximum(jnp.max(jnp.where(valid, past, -jnp.inf), axis=-1), fresh)
-    e_past = jnp.where(valid, jnp.exp(past - top[:, :, None]), 0.0)
-    e_new = jnp.exp(fresh - top)
-    total = jnp.sum(e_past, axis=-1) + e_new
-    p_past = (e_past / total[:, :, None]).astype(bf16)
-    p_new = (e_new / total).astype(bf16)
-    attended = (
-        jnp.einsum("shk,skc->shc", p_past, cache_latent, preferred_element_type=f32)
-        + p_new.astype(f32)[:, :, None] * new_latent.astype(f32)[:, None, :]
-    ).astype(bf16)
-    all_heads = jnp.einsum("shc,cm->shm", attended, w_value, preferred_element_type=f32)
-    own_value = (jnp.arange(heads * VDIM) // VDIM)[None, None, :] == head_ids[None, :, None]
-    values = jnp.sum(jnp.where(own_value, all_heads, 0.0), axis=1).astype(bf16)
-
-    head_rows = lax.all_to_all(values, "ep", split_axis=1, concat_axis=0, tiled=True)
+    whole = pl.BlockSpec(memory_space=pltpu.VMEM)
+    far = pl.BlockSpec(memory_space=pl.ANY)
+    slots_kept = cache_latent.shape[1]
+    values, new_latent, new_rope = pl.pallas_call(
+        attend_kernel,
+        out_shape=(
+            jax.ShapeDtypeStruct((devices, local_seqs, heads * VDIM // devices), bf16),
+            jax.ShapeDtypeStruct((local_seqs, lat_width), bf16),
+            jax.ShapeDtypeStruct((local_seqs, pe_width), bf16),
+        ),
+        in_specs=[whole] * 4 + [pl.BlockSpec(memory_space=pltpu.SMEM)] + [far] * 4,
+        out_specs=(whole, whole, whole),
+        scratch_shapes=[
+            pltpu.VMEM((heads, LANES), f32),
+            pltpu.VMEM(w_absorb.shape, bf16),
+            pltpu.VMEM(w_value.shape, bf16),
+            pltpu.VMEM((pe_width, slots_kept), bf16),
+            pltpu.VMEM((slots_kept, lat_width), bf16),
+            pltpu.SemaphoreType.DMA((4,)),
+        ],
+        name="attend",
+    )(arrived, gain_latent[None], cosine, sine, lengths, w_absorb, w_value, cache_rope, cache_latent)
+
+    head_rows = lax.all_to_all(values, "ep", split_axis=0, concat_axis=0, tiled=True)
+    head_rows = head_rows.reshape(total_rows, -1)
     picked = jnp.dot(sel.reshape(devices * per, total_rows), head_rows,
                      preferred_element_type=f32).astype(bf16)
     out_part = jnp.dot(picked, w_output, preferred_element_type=f32).astype(bf16)
@@ -213,8 +284,6 @@
         out_part.reshape(devices, per, 2, half), "ep", split_axis=0, concat_axis=0, tiled=True
     )
     ff = w_gate.shape[2]
-    whole = pl.BlockSpec(memory_space=pltpu.VMEM)
-    far = pl.BlockSpec(memory_space=pl.ANY)
     resid, spread = pl.pallas_call(
         expert_kernel,
         out_shape=(

time: 87.4 us -> 81.4 us (0.931)
  other arithmetic: 11.8 us -> 4.43 us
  waiting for transfers between devices: 24.2 us -> 30.7 us
  matrix products: 9.02 us -> 2.83 us
  Pallas kernels: 7.1 us -> 13 us
  local copies, waits for them, and re-layouts: 9.37 us -> 6.73 us
  starting transfers between devices: 22.9 us -> 21.6 us
    pallas_call x0 -> x1, Pallas kernels: none -> 5.84 us  [body(): pl.pallas_call(attend_kernel, out_shape=(jax.ShapeDtypeStruct((devices, l...]
    dot_general x6 -> x0, matrix products: 5.22 us -> none  [the longest x1 2.06 us: body(): jnp.einsum('shc,cm->shm', attended, w_value, preferred_element_type=f32)]
    all_to_all x1, waiting for transfers between devices: 4.36 us -> 6.68 us  [body(): lax.all_to_all(partial, 'ep', split_axis=0, concat_axis=0, tiled=True)]
    all_to_all x1, waiting for transfers between devices: 6.56 us -> 8.87 us  [body(): lax.all_to_all(out_part.reshape(devices, per, 2, half), 'ep', split_axis=...]
    concatenate x2 -> x0, other arithmetic: 1.35 us -> none  [apply_rope(): jnp.concatenate([first * cosine - second * sine, second * cosine + first...]
    all_to_all x1, waiting for transfers between devices: 1.63 us -> 2.95 us  [body(): lax.all_to_all(copies, 'ep', split_axis=0, concat_axis=0, tiled=True)]
    squeeze x1, local copies, waits for them, and re-layouts: 1.34 us -> 0.1 us  [body(): sel_mine = lax.dynamic_slice_in_dim(sel, me, 1, axis=0)[0]]
    div x1, other arithmetic: 1.9 us -> 0.68 us  [body(): route_weight = route_scores / jnp.sum(route_scores, axis=-1, keepdims=True)]
  transfers between devices with their start and end apart: 5 -> 5, of which waited for: 5 -> 5; matrix products, arithmetic and copies ran while one was open for 16% -> 9% of each run, Pallas kernels for 0% -> 0%
where the time goes in v3:
time: 81.4 us; the launch traced here: 80.7 us
  waiting for transfers between devices  30.7 us (38%)
  starting transfers between devices  21.6 us (27%)
  Pallas kernels  13 us (16%)
  local copies, waits for them, and re-layouts  6.73 us (8%)
  other arithmetic  4.43 us (5%)
  matrix products  2.83 us (3%)
  between operations  1.46 us (2%)
    all_to_all x1, waiting for transfers between devices, body(): lax.all_to_all(out_part.reshape(devices, per, 2, half), 'ep', split_axis=...  8.87 us
    all_to_all x1, starting transfers between devices, body(): lax.all_to_all(copies, 'ep', split_axis=0, concat_axis=0, tiled=True)  7.41 us
    all_to_all x1, waiting for transfers between devices, body(): lax.all_to_all(partial, 'ep', split_axis=0, concat_axis=0, tiled=True)  6.68 us
    all_to_all x1, waiting for transfers between devices, body(): lax.all_to_all(values, 'ep', split_axis=0, concat_axis=0, tiled=True)  6.17 us
    all_to_all x1, waiting for transfers between devices, body(): lax.all_to_all(spread, 'ep', split_axis=0, concat_axis=0, tiled=True)  6.07 us
    pallas_call x1, Pallas kernels, body(): pl.pallas_call(attend_kernel, out_shape=(jax.ShapeDtypeStruct((devices, l...  5.84 us
    pallas_call x1, Pallas kernels, body(): pl.pallas_call(expert_kernel, out_shape=(jax.ShapeDtypeStruct((local_seqs...  5.07 us
    all_to_all x1, starting transfers between devices, body(): lax.all_to_all(values, 'ep', split_axis=0, concat_axis=0, tiled=True)  3.61 us
  transfers between devices with their start and end apart: 5, of which 5 were waited for; matrix products, arithmetic and copies ran while one was open for 9% of the time, Pallas kernels for 0%

profile of v3, /device:TPU:0, one launch (start us, length us, event | category | flops | bytes accessed | tf_op | source)
XLA Modules:
  0.0 80.7 jit_solution(5518153519723306239)
XLA Ops:
  0.6 0.0 copy-start
  0.6 0.8 reduce.2
  1.4 0.7 reshape.178
  2.1 7.4 %all-to-all-start = ((bf16[16,2,1024]{2,1,0:T(2,128)(2,1)}), bf16[16,2,1024]{2,1,0:T(2,128)(2,1)S(1)}, u32[]{:S(2)}, u32[]{:S(2)}) async-start(bf16[16,2,1024]{2,1,0:T(2,128)(2,1)} %reshape.178), calls=%async_computation | async-start | bytes 131072 | tf_op jit(solution)/shard_map/all_to_all | solution.py:209
  9.5 0.7 convert_element_type.60
  10.2 0.8 %copy.33 = bf16[128,32]{1,0:T(8,128)(2,1)S(1)} copy(bf16[128,32]{0,1:T(8,128)(2,1)} %param.24) | data formatting | bytes 16384 | tf_op args[6]
  11.0 0.6 pad.9.tag_ref
  11.6 0.6 pad.8.wr_ref
  12.2 1.3 %dynamic-slice_bitcast_fusion.gain_ref = f32[1,128]{1,0:T(1,128)} fusion(f32[2048]{0:T(1024)} %param.28, s32[]{:T(128)S(6)} %select_n.18), kind=kLoop, calls=%fused_computation.30 | loop fusion | bytes 1028 | tf_op jit(solution)/shard_map/broadcast_in_dim | solution.py:212
  13.5 3.0 %all-to-all-done = bf16[16,2,1024]{2,1,0:T(2,128)(2,1)S(1)} async-done(((bf16[16,2,1024]{2,1,0:T(2,128)(2,1)}), bf16[16,2,1024]{2,1,0:T(2,128)(2,1)S(1)}, u32[]{:S(2)}, u32[]{:S(2)}) %all-to-all-start) | async-done | bytes 65568 | tf_op jit(solution)/shard_map/all_to_all | solution.py:209
  16.4 0.0 copy-start.2
  16.4 0.6 constant_dynamic-slice_fusion.cols_ref
  17.1 0.0 copy-done.2
  17.1 2.0 %project.1 = f32[16,1,2176]{2,1,0:T(1,128)} custom-call(bf16[16,2048]{1,0:T(8,128)(2,1)} %bitcast.35, bf16[16,128]{1,0:T(8,128)(2,1)} %constant_dynamic-slice_fusion.cols_ref, f32[1,128]{1,0:T(1,128)} %dynamic-slice_bitcast_fusion.gain_ref, bf16[128,1536]{1,0:T(8,128)(2,1)} %wq_ref.1, bf16[128,512]{1,0:T(8,128)(2,1)} %wl_ref.1, bf16[128,128]{1,0:T(8,128)(2,1)} %pad.8.wr_ref, ...), custom_call_target="tpu_custom_call" | custom-call | tf_op jit(solution)/shard_map/project/pallas_call | solution.py:222
  19.1 3.5 %all-to-all-start.1 = ((f32[16,1,2176]{2,1,0:T(1,128)}), f32[16,1,2176]{2,1,0:T(1,128)S(1)}, u32[]{:S(2)}, u32[]{:S(2)}) async-start(f32[16,1,2176]{2,1,0:T(1,128)} %project.1), calls=%async_computation.1 | async-start | bytes 278528 | tf_op jit(solution)/shard_map/all_to_all | solution.py:227
  23.3 0.7 fusion.12
  24.0 6.7 %all-to-all-done.1.part_ref = f32[16,1,2176]{2,1,0:T(1,128)S(1)} async-done(((f32[16,1,2176]{2,1,0:T(1,128)}), f32[16,1,2176]{2,1,0:T(1,128)S(1)}, u32[]{:S(2)}, u32[]{:S(2)}) %all-to-all-start.1) | async-done | bytes 139296 | tf_op jit(solution)/shard_map/all_to_all | solution.py:227
  30.6 0.0 copy-start.4
  30.6 0.1 slice_convert_fusion
  30.7 0.1 copy.34
  30.8 0.1 fusion.1
  30.9 0.1 copy.35
  31.0 0.2 convolution_select_fusion
  31.1 0.1 copy-done.4
  31.3 5.8 %attend.1 = (bf16[16,1,64]{2,1,0:T(2,128)(2,1)}, bf16[1,512]{1,0:T(2,128)(2,1)}, bf16[1,32]{1,0:T(2,128)(2,1)}) custom-call(f32[16,1,2176]{2,1,0:T(1,128)} %copy-done.4, f32[1,512]{1,0:T(1,128)} %bitcast.42, f32[1,16]{1,0:T(1,128)} %get-tuple-element.14.cos_ref, f32[1,16]{1,0:T(1,128)} %get-tuple-element.13.sin_ref, s32[1]{0:T(128)S(6)} %copy.45.len_ref, ...), custom_call_target="tpu_custom_call" | custom-call | tf_op jit(solution)/shard_map/attend/pallas_call | solution.py:258
  37.1 0.0 copy-start.3
  37.1 3.6 %all-to-all-start.2 = ((bf16[16,1,64]{2,1,0:T(2,128)(2,1)}), bf16[16,1,64]{2,1,0:T(2,128)(2,1)S(1)}, u32[]{:S(2)}, u32[]{:S(2)}) async-start(bf16[16,1,64]{2,1,0:T(2,128)(2,1)} %get-tuple-element.8), calls=%async_computation.2 | async-start | bytes 16384 | tf_op jit(solution)/shard_map/all_to_all | solution.py:278
  40.8 0.1 broadcast_compare_fusion
  40.9 6.2 %all-to-all-done.2 = bf16[16,1,64]{2,1,0:T(2,128)(2,1)S(1)} async-done(((bf16[16,1,64]{2,1,0:T(2,128)(2,1)}), bf16[16,1,64]{2,1,0:T(2,128)(2,1)S(1)}, u32[]{:S(2)}, u32[]{:S(2)}) %all-to-all-start.2) | async-done | bytes 2080 | tf_op jit(solution)/shard_map/all_to_all | solution.py:278
  47.1 0.0 copy-done
  47.1 0.5 convolution_convert_fusion
  47.6 1.0 %reshape.182 = bf16[16,5,2,1024]{3,2,1,0:T(2,128)(2,1)} reshape(bf16[80,2048]{1,0:T(8,128)(2,1)S(1)} %convolution_convert_fusion) | data formatting | bytes 655360 | tf_op jit(solution)/shard_map/reshape | solution.py:284
  48.5 3.5 %all-to-all-start.3 = ((bf16[16,5,2,1024]{3,2,1,0:T(2,128)(2,1)}), bf16[16,5,2,1024]{3,2,1,0:T(2,128)(2,1)S(1)}, u32[]{:S(2)}, u32[]{:S(2)}) async-start(bf16[16,5,2,1024]{3,2,1,0:T(2,128)(2,1)} %reshape.182), calls=%async_computation.3 | async-start | bytes 655360 | tf_op jit(solution)/shard_map/all_to_all | solution.py:283
  52.1 0.0 copy-done.5
  52.1 0.7 reduce_sum.18
  52.8 0.1 copy.36
  52.9 0.6 select_bitcast_fusion.pick_ref
  53.5 0.0 copy-done.3
  53.5 0.8 fusion.8.tok_ref
  54.2 8.9 %all-to-all-done.3.parts_ref = bf16[16,5,2,1024]{3,2,1,0:T(2,128)(2,1)S(1)} async-done(((bf16[16,5,2,1024]{3,2,1,0:T(2,128)(2,1)}), bf16[16,5,2,1024]{3,2,1,0:T(2,128)(2,1)S(1)}, u32[]{:S(2)}, u32[]{:S(2)}) %all-to-all-start.3) | async-done | bytes 327712 | tf_op jit(solution)/shard_map/all_to_all | solution.py:283
  63.1 0.7 copy-done.1
  63.8 5.1 %experts.1 = (bf16[1,2048]{1,0:T(2,128)(2,1)}, bf16[16,2,1024]{2,1,0:T(2,128)(2,1)}) custom-call(bf16[16,5,2,1024]{3,2,1,0:T(2,128)(2,1)} %copy-done.1, f32[5,2048]{1,0:T(8,128)} %fusion.8.tok_ref, f32[1,2048]{1,0:T(1,128)} %bitcast.40, bf16[16,5]{1,0:T(8,128)(2,1)} %select_bitcast_fusion.pick_ref, bf16[1,2048,512]{2,1,0:T(8,128)(2,1)} %wg_hbm.1, ...), custom_call_target="tpu_custom_call" | custom-call | tf_op jit(solution)/shard_map/experts/pallas_call | solution.py:287
  68.9 3.5 %all-to-all-start.4 = ((bf16[16,2,1024]{2,1,0:T(2,128)(2,1)}), bf16[16,2,1024]{2,1,0:T(2,128)(2,1)S(1)}, u32[]{:S(2)}, u32[]{:S(2)}) async-start(bf16[16,2,1024]{2,1,0:T(2,128)(2,1)} %get-tuple-element.10), calls=%async_computation.4 | async-start | bytes 131072 | tf_op jit(solution)/shard_map/all_to_all | solution.py:304
  72.4 0.7 divide_bitcast_fusion
  73.1 0.0 copy-done.6
  73.1 0.1 fusion.10
  73.2 6.1 %all-to-all-done.4 = bf16[16,2,1024]{2,1,0:T(2,128)(2,1)S(1)} async-done(((bf16[16,2,1024]{2,1,0:T(2,128)(2,1)}), bf16[16,2,1024]{2,1,0:T(2,128)(2,1)S(1)}, u32[]{:S(2)}, u32[]{:S(2)}) %all-to-all-start.4) | async-done | bytes 65568 | tf_op jit(solution)/shard_map/all_to_all | solution.py:304
  79.3 1.4 %fusion = bf16[1,2048]{1,0:T(2,128)(2,1)} fusion(bf16[16,2048]{1,0:T(8,128)(2,1)S(1)} %bitcast.39, bf16[1,2048]{1,0:T(2,128)(2,1)} %get-tuple-element.9, bf16[16]{0:T(256)(128)(2,1)S(1)} %fusion.10), kind=kOutput, calls=%fused_computation.2 | convolution fusion | flops 71680 | bytes 73760 | tf_op jit(solution)/shard_map/sn,nsd->sd/dot_general | solution.py:306
  (12 shorter events, 0.1 us)
Async XLA Ops:
  0.6 46.5 %copy-start = (bf16[64,2048]{1,0:T(8,128)(2,1)S(1)}, bf16[64,2048]{1,0:T(8,128)(2,1)}, u32[]{:S(2)}) copy-start(bf16[64,2048]{1,0:T(8,128)(2,1)} %param.27) | copy-start | bytes 786436
  2.1 14.3 %all-to-all-start = ((bf16[16,2,1024]{2,1,0:T(2,128)(2,1)}), bf16[16,2,1024]{2,1,0:T(2,128)(2,1)S(1)}, u32[]{:S(2)}, u32[]{:S(2)}) async-start(bf16[16,2,1024]{2,1,0:T(2,128)(2,1)} %reshape.178), calls=%async_computation | async-start | bytes 131072 | tf_op jit(solution)/shard_map/all_to_all | solution.py:209
  16.4 0.6 copy-start.2
  19.1 11.5 %all-to-all-start.1 = ((f32[16,1,2176]{2,1,0:T(1,128)}), f32[16,1,2176]{2,1,0:T(1,128)S(1)}, u32[]{:S(2)}, u32[]{:S(2)}) async-start(f32[16,1,2176]{2,1,0:T(1,128)} %project.1), calls=%async_computation.1 | async-start | bytes 278528 | tf_op jit(solution)/shard_map/all_to_all | solution.py:227
  30.6 0.7 copy-start.4
  31.3 20.8 %copy-start.5 = (f32[1,2]{1,0:T(1,128)S(1)}, f32[1,2]{1,0:T(1,128)}, u32[]{:S(2)}) copy-start(f32[1,2]{1,0:T(1,128)} %param.32) | copy-start | bytes 28
  37.1 16.3 %copy-start.3 = (bf16[2,8,2,1024]{3,1,2,0:T(8,128)(2,1)S(1)}, bf16[2,8,2,1024]{3,1,2,0:T(8,128)(2,1)}, u32[]{:S(2)}) copy-start(bf16[2,8,2,1024]{3,1,2,0:T(8,128)(2,1)} %copy-done.2) | copy-start | bytes 196612
  37.1 9.9 %all-to-all-start.2 = ((bf16[16,1,64]{2,1,0:T(2,128)(2,1)}), bf16[16,1,64]{2,1,0:T(2,128)(2,1)S(1)}, u32[]{:S(2)}, u32[]{:S(2)}) async-start(bf16[16,1,64]{2,1,0:T(2,128)(2,1)} %get-tuple-element.8), calls=%async_computation.2 | async-start | bytes 16384 | tf_op jit(solution)/shard_map/all_to_all | solution.py:278
  48.5 14.6 %all-to-all-start.3 = ((bf16[16,5,2,1024]{3,2,1,0:T(2,128)(2,1)}), bf16[16,5,2,1024]{3,2,1,0:T(2,128)(2,1)S(1)}, u32[]{:S(2)}, u32[]{:S(2)}) async-start(bf16[16,5,2,1024]{3,2,1,0:T(2,128)(2,1)} %reshape.182), calls=%async_computation.3 | async-start | bytes 655360 | tf_op jit(solution)/shard_map/all_to_all | solution.py:283
  63.1 0.7 copy-start.1
  63.8 9.3 %copy-start.6 = (s32[1,2]{1,0:T(1,128)S(1)}, s32[1,2]{1,0:T(1,128)}, u32[]{:S(2)}) copy-start(s32[1,2]{1,0:T(1,128)} %param.31) | copy-start | bytes 28
  68.9 10.4 %all-to-all-start.4 = ((bf16[16,2,1024]{2,1,0:T(2,128)(2,1)}), bf16[16,2,1024]{2,1,0:T(2,128)(2,1)S(1)}, u32[]{:S(2)}, u32[]{:S(2)}) async-start(bf16[16,2,1024]{2,1,0:T(2,128)(2,1)} %get-tuple-element.10), calls=%async_computation.4 | async-start | bytes 131072 | tf_op jit(solution)/shard_map/all_to_all | solution.py:304
